TPU v7x, 512 devices: a whole 4x8x8 slice. The times are simulated.
512 devices in a mesh: ep: 32 (over z, x), tp: 16 (over y, core).
Axes of the slice: x: 4, y: 8, z: 8, core: 2. Of those that a mesh axis runs over, the one named last changes fastest.
Arguments:
- queries: bfloat16 [4096, 4096], P('ep', 'tp'), may hold values from -112 to 112
- key_rows: bfloat16 [4096, 4096], P('ep', 'tp'), may hold values from -8.1 to 8.1
- values: bfloat16 [4096, 4096], P('ep', 'tp'), may hold values from -6 to 6
- lambdas: float32 [16], P('tp'), may hold values from 0.3 to 0.8
- head_gain: float32 [256], replicated, may hold values from 0.1 to 1.9
- tokens: bfloat16 [2048, 4096], P('ep'), may hold values from -6 to 6
- moe_gain: float32 [4096], replicated, may hold values from 0.1 to 1.9
- routes: int32 [2048, 2], P('ep'), may hold values from 0 to 31, all different within a row; in each aligned block of 64 rows (0 to 63, 64 to 127, ...) at most 8 rows name the same one
- route_scores: float32 [2048, 2], P('ep'), may hold values from -6 to 6
- w_gate: bfloat16 [32, 4096, 2048], P('ep', None, 'tp'), may hold values from -0.09375 to 0.09375
- w_up: bfloat16 [32, 4096, 2048], P('ep', None, 'tp'), may hold values from -0.09375 to 0.09375
- w_down: bfloat16 [32, 2048, 4096], P('ep', 'tp'), may hold values from -0.125 to 0.125
Outputs:
- attended: bfloat16 [4096, 4096], P('ep', 'tp')
- expert_out: bfloat16 [2048, 4096], P('ep', 'tp')
Inputs may be any that keep to these rules, and one draw needn't show every extreme that they name: `routes`: each row names 2 different experts. Among the rows of one index of ep at most 8 name the same expert, and some index reaches 8 in every draw.
All inputs are finite; a program needn't handle non-finite values.
Results may differ from a plain program's by a relative error of at most 0.018.
Values may be sent and summed in bfloat16 or wider, within the bound.
A program may use at most 64 MiB of HBM per device.

v0:
```python
import jax
import jax.numpy as jnp
from jax import lax
from jax.sharding import PartitionSpec as P

QKD = 128
VD = 256
TOP = 2


neg_big = -1e30
head_eps = 1e-05
moe_eps = 1e-06
head_scale = 0.8


def sent_together(arrays, axis, dim, along):
    widths = [a.shape[along] for a in arrays]
    both = jnp.concatenate(arrays, axis=along)
    whole = lax.all_gather(both, axis, axis=dim, tiled=True)
    return tuple(jnp.split(whole, [sum(widths[:k]) for k in range(1, len(widths))], axis=along))


def split_up(value, dim, peers):
    before, after = (value.shape[:dim], value.shape[dim + 1 :])
    return jnp.moveaxis(value.reshape(*before, peers, -1, *after), dim, 0)


def sent_and_summed(value, axis, dim):
    pieces = split_up(value, dim, lax.axis_size(axis))
    arrived = lax.all_to_all(pieces, axis, split_axis=0, concat_axis=0, tiled=True)
    return arrived.astype(jnp.float32).sum(axis=0)


def slot_table(routes, experts, capacity):
    flat_routes = routes.reshape(-1)
    onehot = (flat_routes[:, None] == jnp.arange(experts, dtype=jnp.int32)[None, :]).astype(
        jnp.int32
    )
    before = jnp.cumsum(onehot, axis=0) - onehot
    position = jnp.sum(before * onehot, axis=1)
    return (flat_routes * capacity + position).reshape(routes.shape)


def fold_block(state, query_group, query_pos, key_heads, value_heads, key_pos):
    maxima, denominators, accumulated = state
    scores = jnp.einsum(
        "qhmd,khmd->hmqk", query_group, key_heads, preferred_element_type=jnp.float32
    ) * QKD ** (-0.5)
    visible = key_pos[None, :] <= query_pos[:, None]
    scores = jnp.where(visible, scores, neg_big)
    new_max = jnp.maximum(maxima, jnp.max(scores, axis=-1))
    weights = jnp.where(visible, jnp.exp(scores - new_max[..., None]), 0.0)
    accumulated = jnp.einsum("hmqk,khd->hmqd", weights, value_heads)
    denominators = jnp.sum(weights, axis=-1)
    return (new_max, denominators, accumulated)


def local(
    queries,
    key_rows,
    values,
    lambdas,
    head_gain,
    tokens,
    moe_gain,
    routes,
    route_scores,
    w_gate,
    w_up,
    w_down,
):
    rows_a = queries.shape[0]
    half_rows = rows_a // 2
    head_local = lambdas.shape[0]
    ep_count = lax.axis_size("ep")
    ep_index = lax.axis_index("ep")
    early_queries = queries[:half_rows]
    later_queries = queries[half_rows:]
    early_pos = ep_index * rows_a + jnp.arange(half_rows, dtype=jnp.int32)
    later_pos = ep_index * rows_a + half_rows + jnp.arange(half_rows, dtype=jnp.int32)
    query_groups = (
        early_queries.reshape(half_rows, head_local, 2, QKD),
        later_queries.reshape(half_rows, head_local, 2, QKD),
    )
    position_groups = (early_pos, later_pos)
    start_state = (
        jnp.full((head_local, 2, half_rows), neg_big, jnp.float32),
        jnp.zeros((head_local, 2, half_rows), jnp.float32),
        jnp.zeros((head_local, 2, half_rows, VD), jnp.float32),
    )
    totals = (start_state, start_state)
    row_start = jnp.int32(0)
    key_block, value_block = sent_together((key_rows, values), "ep", 0, 1)
    key_count = key_block.shape[0]
    key_heads = key_block.reshape(key_count, head_local, 2, QKD)
    value_heads = value_block.reshape(key_count, head_local, VD).astype(jnp.float32)
    key_pos = jnp.arange(key_count, dtype=jnp.int32)
    updated = []
    for attend_group_index in range(2):
        state = totals[attend_group_index]
        query_group = query_groups[attend_group_index]
        query_pos = position_groups[attend_group_index]
        state = lax.cond(
            row_start <= query_pos[-1],
            lambda held: fold_block(held, query_group, query_pos, key_heads, value_heads, key_pos),
            lambda held: held,
            state,
        )
        updated.append(state)
    folded = (updated[0], updated[1])
    attended_groups = []
    for group_index in range(2):
        maxima, denominators, accumulated = folded[group_index]
        mixed_out = (
            accumulated[:, 0] / denominators[:, 0, :, None]
            - lambdas[:, None, None] * accumulated[:, 1] / denominators[:, 1, :, None]
        )
        scaled = mixed_out * lax.rsqrt(
            jnp.mean(mixed_out * mixed_out, axis=-1, keepdims=True) + head_eps
        )
        scaled = scaled * head_gain * head_scale
        attended_groups.append(
            scaled.transpose(1, 0, 2).reshape(half_rows, head_local * VD).astype(jnp.bfloat16)
        )
    later_out = attended_groups[1]
    attended = jnp.concatenate([attended_groups[0], later_out], axis=0)
    rows_b = tokens.shape[0]
    capacity = 2 * TOP * rows_b // ep_count
    token_f32 = tokens.astype(jnp.float32)
    normed = (
        token_f32
        * lax.rsqrt(jnp.mean(token_f32 * token_f32, axis=-1, keepdims=True) + moe_eps)
        * moe_gain
    ).astype(jnp.bfloat16)
    gate_weights = jax.nn.softmax(route_scores, axis=-1)
    slot_of = slot_table(routes, ep_count, capacity)
    row_ids = jnp.broadcast_to(jnp.arange(rows_b, dtype=jnp.int32)[:, None], slot_of.shape)
    row_of_slot = (
        jnp.zeros((ep_count * capacity,), jnp.int32)
        .at[slot_of.reshape(-1)]
        .set(row_ids.reshape(-1))
    )
    gate_local = w_gate[0]
    up_local = w_up[0]
    down_local = w_down[0]
    outgoing = normed[row_of_slot]
    arrived = lax.all_to_all(outgoing, "ep", split_axis=0, concat_axis=0, tiled=True)
    gate_act = jnp.dot(arrived, gate_local, preferred_element_type=jnp.float32)
    up_act = jnp.dot(arrived, up_local, preferred_element_type=jnp.float32)
    hidden = (jax.nn.silu(gate_act) * up_act).astype(jnp.bfloat16)
    summed = sent_and_summed(
        lax.dot_general(
            down_local, hidden, (((0,), (1,)), ((), ())), preferred_element_type=jnp.float32
        ).astype(jnp.bfloat16),
        "tp",
        0,
    )
    expert_rows = summed.astype(jnp.bfloat16)
    returned = lax.all_to_all(expert_rows, "ep", split_axis=1, concat_axis=1, tiled=True)
    slot_ids = jnp.arange(ep_count * capacity, dtype=jnp.int32)
    combined = jnp.zeros((rows_b, returned.shape[0]), jnp.float32)
    for choice_index in range(TOP):
        picker = (slot_of[:, choice_index, None] == slot_ids[None, :]).astype(jnp.bfloat16)
        picked = lax.dot_general(
            picker, returned, (((1,), (1,)), ((), ())), preferred_element_type=jnp.float32
        )
        combined = combined + gate_weights[:, choice_index, None] * picked
    expert_out = combined.astype(jnp.bfloat16)
    return (attended, expert_out)


def solution(mesh):
    return jax.shard_map(
        local,
        mesh=mesh,
        in_specs=(
            P("ep", "tp"),
            P("ep", "tp"),
            P("ep", "tp"),
            P("tp"),
            P(),
            P("ep", None),
            P(),
            P("ep", None),
            P("ep", None),
            P("ep", None, "tp"),
            P("ep", None, "tp"),
            P("ep", "tp", None),
        ),
        out_specs=(P("ep", "tp"), P("ep", "tp")),
        check_vma=False,
    )
```

profile of v0, /device:TPU:1, one launch (start us, length us, event | category | flops | bytes accessed | tf_op | source)
XLA Modules:
  0.0 182.0 jit_solution(8576443605019141647)
XLA Ops:
  7.2 0.0 copy-start
  7.2 0.9 copy.34
  8.0 0.1 eq.45
  8.2 0.1 fusion.70
  8.3 0.2 reduce_window_sum.11
  8.4 0.2 select_reduce_fusion
  8.6 0.1 reduce_sum.87
  8.8 0.1 mul.234
  8.9 0.1 reshape.456
  9.1 1.0 scatter_custom_fusion
  10.1 1.2 fusion.43
  11.4 1.2 fusion.45
  12.6 3.2 %gather_fusion = bf16[256,4096]{1,0:T(8,128)(2,1)} fusion(bf16[64,4096]{1,0:T(8,128)(2,1)S(1)} %fusion.45, s32[1024]{0:T(1024)S(1)} %pad_clamp_fusion), kind=kCustom, calls=%fused_computation | custom fusion | bytes 4195328 | tf_op jit(solution)/shard_map/gather | solution.py:147
  15.8 0.0 copy-start.1
  15.8 0.0 copy-start.2
  15.8 13.8 %all-to-all-start = ((bf16[32,8,4096]{2,1,0:T(8,128)(2,1)}), bf16[32,8,4096]{2,1,0:T(8,128)(2,1)S(1)}, u32[]{:S(2)}, u32[]{:S(2)}) async-start(bf16[32,8,4096]{2,1,0:T(8,128)(2,1)} %bitcast.190), calls=%async_computation | async-start | bytes 4194304 | tf_op jit(solution)/shard_map/all_to_all | solution.py:148
  29.6 0.0 all-gather.2.cloned.1.call-start
  29.7 0.0 copy-done.1
  29.7 0.1 copy.28
  29.8 0.0 copy-done.2
  29.8 0.1 copy.29
  29.9 0.7 pad_maximum_fusion
  30.6 0.0 all-gather.2.cloned.1.call-update
  30.6 50.9 %all-to-all-done = bf16[32,8,4096]{2,1,0:T(8,128)(2,1)S(1)} async-done(((bf16[32,8,4096]{2,1,0:T(8,128)(2,1)}), bf16[32,8,4096]{2,1,0:T(8,128)(2,1)S(1)}, u32[]{:S(2)}, u32[]{:S(2)}) %all-to-all-start) | async-done | bytes 2097184 | tf_op jit(solution)/shard_map/all_to_all | solution.py:148
  81.6 1.9 %fusion.31 = f32[256,128]{1,0:T(8,128)S(1)} fusion(bf16[32,8,4096]{2,1,0:T(8,128)(2,1)S(1)} %all-to-all-done, bf16[1,4096,128]{2,1,0:T(8,128)(2,1)} %param.25), kind=kOutput, calls=%fused_computation.46 | convolution fusion | flops 268435456 | bytes 3276800 | tf_op jit(solution)/shard_map/dot_general | solution.py:149
  83.5 0.0 copy-done
  83.5 3.9 %convolution_convert_fusion = bf16[256,4096]{1,0:T(8,128)(2,1)} fusion(bf16[32,8,4096]{2,1,0:T(8,128)(2,1)S(1)} %all-to-all-done, bf16[1,128,4096]{2,1,0:T(8,128)(2,1)S(1)} %copy-done, bf16[1,4096,128]{2,1,0:T(8,128)(2,1)} %param.26, f32[256,128]{1,0:T(8,128)S(1)} %fusion.31), kind=kOutput, calls=%fused_computation.40 | convolution fusion | flops 538116096 | bytes 6422528 | tf_op jit(solution)/shard_map/dot_general | solution.py:153
  87.4 3.1 %copy.59 = bf16[32,16,8,256]{3,2,0,1:T(8,128)(2,1)} copy(bf16[32,16,8,256]{3,2,1,0:T(8,128)(2,1)} %bitcast.191) | data formatting | bytes 4194304 | tf_op jit(solution)/shard_map/reshape | solution.py:26
  90.5 0.0 copy-start.4
  90.5 11.2 %all-to-all-start.1 = ((bf16[16,256,256]{1,2,0:T(8,128)(2,1)}), bf16[16,256,256]{1,2,0:T(8,128)(2,1)S(1)}, u32[]{:S(2)}, u32[]{:S(2)}) async-start(bf16[16,256,256]{1,2,0:T(8,128)(2,1)} %bitcast.192), calls=%async_computation.1 | async-start | bytes 4194304 | tf_op jit(solution)/shard_map/all_to_all | solution.py:31
  101.7 0.6 slice.71
  102.9 0.0 copy-start.7
  102.9 0.6 slice.68
  104.2 0.0 copy-done.7
  104.8 0.0 copy-done.4
  104.9 0.7 slice_reduce_fusion
  105.6 0.5 slice_bitcast_fusion.7
  106.2 44.6 %all-to-all-done.1 = bf16[16,256,256]{1,2,0:T(8,128)(2,1)S(1)} async-done(((bf16[16,256,256]{1,2,0:T(8,128)(2,1)}), bf16[16,256,256]{1,2,0:T(8,128)(2,1)S(1)}, u32[]{:S(2)}, u32[]{:S(2)}) %all-to-all-start.1) | async-done | bytes 2097184 | tf_op jit(solution)/shard_map/all_to_all | solution.py:31
  150.7 1.0 reduce_sum.90
  151.7 5.1 %all-to-all-start.2 = ((bf16[256,32,8]{0,2,1:T(8,128)(2,1)}), bf16[256,32,8]{0,2,1:T(8,128)(2,1)S(1)}, u32[]{:S(2)}, u32[]{:S(2)}) async-start(bf16[256,32,8]{0,2,1:T(8,128)(2,1)} %bitcast.37), calls=%async_computation.2 | async-start | bytes 262144 | tf_op jit(solution)/shard_map/all_to_all | solution.py:160
  156.8 0.0 copy-start.3
  156.8 0.0 all-gather.2.cloned.1.call-done
  156.9 3.9 %fusion.28 = (bf16[4096,1,256]{0,2,1:T(8,128)(2,1)}, bf16[4096,256]{0,1:T(8,128)(2,1)S(1)}) fusion(bf16[4096,512]{0,1:T(8,128)(2,1)} %all-gather.2.cloned.1.call-done), kind=kLoop, calls=%fused_computation.43 | loop fusion | bytes 8388608 | tf_op jit(solution)/shard_map/convert_element_type | solution.py:97
  160.8 0.0 copy-done.3
  160.8 4.2 %conditional.3 = (f32[64]{0:T(128)S(1)}, f32[64]{0:T(128)S(1)}, f32[1,1,64,256]{3,2,1,0:T(8,128)S(1)}, f32[1,1,64,256]{3,2,1,0:T(8,128)S(1)}) conditional(s32[]{:T(128)} %bitcast.22, () %tuple.38, (s32[4096]{0:T(1024)S(1)}, s32[64]{0:T(128)S(1)}, bf16[128,256]{1,0:T(8,128)(2,1)S(1)}, bf16[4096,1,2,128]{0,3,2,1:T(8,128)(2,1)S(1)}, ...), branch_computations={%region_5.6_spmd.clone, %region_6.9_spmd.clone} | conditional | flops 407109504 | bytes 11981088 | solution.py:104
  160.8 0.2 broadcast_compare_fusion.1
  161.1 0.8 fusion.87
  161.8 2.5 %fusion.19 = f32[1,2,64,256]{3,2,1,0:T(8,128)S(1)} fusion(bf16[4096,1,256]{0,2,1:T(8,128)(2,1)} %get-tuple-element.123, f32[2,64,4096]{2,1,0:T(8,128)S(1)} %get-tuple-element.141, f32[2,64]{1,0:T(2,128)S(1)} %broadcast_maximum_fusion.1, pred[64,4096]{1,0:T(8,128)(4,1)S(1)} %broadcast_compare_fusion.1), kind=kOutput, calls=%fused_computation.28 | convolution fusion | flops 269484032 | bytes 4588032 | tf_op jit(solution)/shard_map/cond/branch_1_fun/hmqk,khd->hmqd/dot_general | solution.py:54
  164.4 0.7 fusion.18
  165.0 0.0 copy-start.5
  165.0 0.0 copy-start.6
  165.1 0.5 copy-done.5
  165.6 0.1 copy-done.6
  165.6 4.9 %conditional.2 = (f32[64]{0:T(128)S(1)}, f32[64]{0:T(128)S(1)}, f32[1,1,64,256]{3,2,1,0:T(8,128)S(1)}, f32[1,1,64,256]{3,2,1,0:T(8,128)S(1)}) conditional(s32[]{:T(128)} %bitcast.14, () %tuple.36, (s32[4096]{0:T(1024)S(1)}, s32[64]{0:T(128)}, bf16[128,256]{1,0:T(8,128)(2,1)S(1)}, bf16[4096,1,2,128]{0,3,2,1:T(8,128)(2,1)S(1)}, ...), branch_computations={%region_0.0_spmd.clone, %region_1.4_spmd.clone} | conditional | flops 407109504 | bytes 11981088 | solution.py:104
  165.6 0.9 broadcast_compare_fusion
  166.5 0.8 fusion.85
  167.3 2.5 %fusion.5 = f32[1,2,64,256]{3,2,1,0:T(8,128)S(1)} fusion(bf16[4096,1,256]{0,2,1:T(8,128)(2,1)} %get-tuple-element.110, f32[2,64,4096]{2,1,0:T(8,128)S(1)} %get-tuple-element.135, f32[2,64]{1,0:T(2,128)S(1)} %broadcast_maximum_fusion, pred[64,4096]{1,0:T(8,128)(4,1)S(1)} %broadcast_compare_fusion), kind=kOutput, calls=%fused_computation.9 | convolution fusion | flops 269484032 | bytes 4588032 | tf_op jit(solution)/shard_map/cond/branch_1_fun/hmqk,khd->hmqd/dot_general | solution.py:54
  169.8 0.7 fusion.4
  170.5 0.9 fusion.73
  171.4 0.8 fusion.71
  172.2 0.6 pad_maximum_fusion.1
  172.9 0.0 all-to-all-done.2
  172.9 0.8 convolution_multiply_fusion.3
  173.7 1.4 fusion.42
  (21 shorter events, 0.2 us)
Async XLA Ops:
  7.2 76.3 %copy-start = (bf16[1,128,4096]{2,1,0:T(8,128)(2,1)S(1)}, bf16[1,128,4096]{2,1,0:T(8,128)(2,1)}, u32[]{:S(2)}) copy-start(bf16[1,128,4096]{2,1,0:T(8,128)(2,1)} %param.27) | copy-start | bytes 3145732
  15.8 13.9 %copy-start.1 = (bf16[128,256]{1,0:T(8,128)(2,1)S(1)}, bf16[128,256]{1,0:T(8,128)(2,1)}, u32[]{:S(2)}) copy-start(bf16[128,256]{1,0:T(8,128)(2,1)} %param.17) | copy-start | bytes 196612
  15.8 14.0 %copy-start.2 = (bf16[128,256]{1,0:T(8,128)(2,1)S(1)}, bf16[128,256]{1,0:T(8,128)(2,1)}, u32[]{:S(2)}) copy-start(bf16[128,256]{1,0:T(8,128)(2,1)} %param.18) | copy-start | bytes 196612
  15.8 65.8 %all-to-all-start = ((bf16[32,8,4096]{2,1,0:T(8,128)(2,1)}), bf16[32,8,4096]{2,1,0:T(8,128)(2,1)S(1)}, u32[]{:S(2)}, u32[]{:S(2)}) async-start(bf16[32,8,4096]{2,1,0:T(8,128)(2,1)} %bitcast.190), calls=%async_computation | async-start | bytes 4194304 | tf_op jit(solution)/shard_map/all_to_all | solution.py:148
  29.6 127.2 %all-gather.2.cloned.1.call-start = ((), (), s32[]{:S(2)}) async-start(), calls=%async_computation.3 | async-start | bytes 4325376 | tf_op jit(solution)/shard_map/all_gather | solution.py:20
  90.5 14.3 %copy-start.4 = (f32[64,2]{0,1:T(2,128)S(1)}, f32[64,2]{0,1:T(2,128)}, u32[]{:S(2)}) copy-start(f32[64,2]{0,1:T(2,128)} %param.24) | copy-start | bytes 1540
  90.5 60.2 %all-to-all-start.1 = ((bf16[16,256,256]{1,2,0:T(8,128)(2,1)}), bf16[16,256,256]{1,2,0:T(8,128)(2,1)S(1)}, u32[]{:S(2)}, u32[]{:S(2)}) async-start(bf16[16,256,256]{1,2,0:T(8,128)(2,1)} %bitcast.192), calls=%async_computation.1 | async-start | bytes 4194304 | tf_op jit(solution)/shard_map/all_to_all | solution.py:31
  102.9 1.2 copy-start.7
  151.7 21.2 %all-to-all-start.2 = ((bf16[256,32,8]{0,2,1:T(8,128)(2,1)}), bf16[256,32,8]{0,2,1:T(8,128)(2,1)S(1)}, u32[]{:S(2)}, u32[]{:S(2)}) async-start(bf16[256,32,8]{0,2,1:T(8,128)(2,1)} %bitcast.37), calls=%async_computation.2 | async-start | bytes 262144 | tf_op jit(solution)/shard_map/all_to_all | solution.py:160
  156.8 4.0 %copy-start.3 = (bf16[128,256]{1,0:T(8,128)(2,1)S(1)}, bf16[128,256]{1,0:T(8,128)(2,1)}, u32[]{:S(2)}) copy-start(bf16[128,256]{1,0:T(8,128)(2,1)} %param.16) | copy-start | bytes 196612
  165.0 0.5 copy-start.5
  165.0 0.6 copy-start.6
Sparse Core Ops, SparseCore 0:
  33.5 98.2 all-gather.1
where the time goes:
time: 183 us; the launch traced here: 182 us
  waiting for transfers between devices  95.5 us (52%)
  starting transfers between devices  30.2 us (17%)
  between operations  16.2 us (9%)
  local copies, waits for them, and re-layouts  16 us (9%)
  matrix products  14.6 us (8%)
  other arithmetic  9.36 us (5%)
    all_to_all x1, waiting for transfers between devices, local(): lax.all_to_all(outgoing, 'ep', split_axis=0, concat_axis=0, tiled=True)  50.9 us
    all_to_all x1, waiting for transfers between devices, sent_and_summed(): lax.all_to_all(pieces, axis, split_axis=0, concat_axis=0, tiled=True)  44.6 us
    all_to_all x1, starting transfers between devices, local(): lax.all_to_all(outgoing, 'ep', split_axis=0, concat_axis=0, tiled=True)  13.8 us
    all_to_all x1, starting transfers between devices, sent_and_summed(): lax.all_to_all(pieces, axis, split_axis=0, concat_axis=0, tiled=True)  11.2 us
    all_to_all x1, starting transfers between devices, local(): lax.all_to_all(expert_rows, 'ep', split_axis=1, concat_axis=1, tiled=True)  5.15 us
    dot_general x2, matrix products, fold_block(): accumulated = jnp.einsum('hmqk,khd->hmqd', weights, value_heads)  5.05 us
    convert_element_type x1, local copies, waits for them, and re-layouts, local(): value_block.reshape(key_count, head_local, VD).astype(jnp.float32)  3.94 us
    dot_general x1, matrix products, local(): lax.dot_general(down_local, hidden, (((0,), (1,)), ((), ())), preferred_e...  3.89 us
  transfers between devices with their start and end apart: 4, of which 2 were waited for; matrix products, arithmetic and copies ran while one was open for 16% of the time, Pallas kernels for 0%

commit v1 on v0

v1 whole, which is shorter than its diff:
```python
import jax
import jax.numpy as jnp
from jax import lax
from jax.experimental import pallas as pl
from jax.experimental.pallas import tpu as pltpu
from jax.sharding import PartitionSpec as P

MESH = pl.DeviceIdType.MESH
F32 = jnp.float32
BF16 = jnp.bfloat16

QKD = 128
VD = 256
D = 4096
N_EP = 32
N_TP = 16
NX = 4
RING = 8
CAP = 8
ROWS_A = 128
ROWS_B = 64
SLOTS = N_EP * CAP
FEAT = D // N_TP
FFL = 128
SUB = 4
SROWS = SLOTS // SUB
KSUB = 2
KROWS = ROWS_A // KSUB

neg_big = -1e30
head_eps = 1e-05
moe_eps = 1e-06
head_scale = 0.8


def kernel(
    q_in, k_in, v_in, lam_in, hg_in, tok_in, mg_in, routes_in, rs_in, wg_in, wu_in, wd_in,
    att_out, exp_out,
    tok, small_sem, wsem, outbox, inbox, gath, wgu, wdx, hid, zown, sbuf, rbuf,
    ebox, retbox, qall, kv, osend, ssend, orecv, srecv,
    disp_s, disp_r, ag_s, ag_r, dd_s, dd_r, wdx_s, wdx_r, hid_s, hid_r,
    rsc_s, rsc_r, ret_s, ret_r, q_s, q_r, kv_s, kv_r, o_s, o_r,
):
    ep = lax.axis_index("ep")
    tp = lax.axis_index("tp")
    z, x = lax.div(ep, NX), lax.rem(ep, NX)
    y, core = lax.div(tp, 2), lax.rem(tp, 2)
    mate = (ep, y * 2 + 1 - core)

    def ring(i, d):
        return lax.rem(i + d + RING, RING)

    y_next = ((ep, ring(y, 1) * 2 + core), (ep, ring(y, -1) * 2 + core))
    z_next = ((ring(z, 1) * NX + x, tp), (ring(z, -1) * NX + x, tp))

    def ep_peer(k):
        return lax.rem(ep + k, N_EP)

    def x_peer(k):
        return z * NX + lax.rem(x + k, NX)

    def rdma(src, dst, ssem, rsem, dev):
        return pltpu.make_async_remote_copy(
            src_ref=src, dst_ref=dst, send_sem=ssem, recv_sem=rsem,
            device_id=dev, device_id_type=MESH,
        )

    tok_load = pltpu.make_async_copy(tok_in, tok, small_sem.at[0])
    tok_load.start()
    loads_q = pltpu.make_async_copy(q_in, qall.at[x], small_sem.at[1])
    loads_k = pltpu.make_async_copy(k_in, kv.at[z, :, pl.ds(0, 256)], small_sem.at[2])
    loads_v = pltpu.make_async_copy(v_in, kv.at[z, :, pl.ds(256, 256)], small_sem.at[3])
    loads_q.start()
    loads_k.start()
    loads_v.start()
    load_wg = pltpu.make_async_copy(wg_in.at[0], wgu.at[:, pl.ds(0, FFL)], wsem.at[0])
    load_wu = pltpu.make_async_copy(wu_in.at[0], wgu.at[:, pl.ds(FFL, FFL)], wsem.at[1])
    load_wg.start()
    load_wu.start()

    def wd_cols(yd, c):
        return wd_in.at[0, :, pl.ds(pl.multiple_of((yd * 2 + c) * FEAT, FEAT), FEAT)]

    def wd_load(yd):
        return pltpu.make_async_copy(wd_cols(yd, core), wdx.at[core, yd], wsem.at[2 + yd])

    for yd in range(RING):
        wd_load(yd).start()

    barrier = pltpu.get_barrier_semaphore()

    def greet(k, carry):
        pl.semaphore_signal(barrier, inc=1, device_id=(ep_peer(k), tp), device_id_type=MESH)
        return carry

    lax.fori_loop(1, N_EP, greet, 0)
    for dev in (*y_next, mate):
        pl.semaphore_signal(barrier, inc=1, device_id=dev, device_id_type=MESH)

    r0, r1 = routes_in[:, 0:1], routes_in[:, 1:2]
    lane = lax.broadcasted_iota(jnp.int32, (ROWS_B, 128), 1)
    hit0, hit1 = lane == r0, lane == r1
    named = jnp.where(hit0 | hit1, 1.0, 0.0).astype(BF16)
    row_i = lax.broadcasted_iota(jnp.int32, (ROWS_B, ROWS_B), 0)
    col_i = lax.broadcasted_iota(jnp.int32, (ROWS_B, ROWS_B), 1)
    earlier = jnp.where(col_i < row_i, 1.0, 0.0).astype(BF16)
    before = jnp.dot(earlier, named, preferred_element_type=F32)
    pos0 = jnp.sum(jnp.where(hit0, before, 0.0), axis=1, keepdims=True)
    pos1 = jnp.sum(jnp.where(hit1, before, 0.0), axis=1, keepdims=True)
    slot0 = r0.astype(F32) * CAP + pos0
    slot1 = r1.astype(F32) * CAP + pos1
    slot_lane = lax.broadcasted_iota(jnp.int32, (ROWS_B, SLOTS), 1).astype(F32)
    pick0 = jnp.where(slot_lane == slot0, 1.0, 0.0)
    pick1 = jnp.where(slot_lane == slot1, 1.0, 0.0)
    s0, s1 = rs_in[:, 0:1], rs_in[:, 1:2]
    smax = jnp.maximum(s0, s1)
    g0, g1 = jnp.exp(s0 - smax), jnp.exp(s1 - smax)
    gsum = g0 + g1
    g0, g1 = g0 / gsum, g1 / gsum

    tok_load.wait()
    squares = jnp.zeros((ROWS_B, 256), F32)
    for i in range(D // 256):
        part = tok[:, i * 256:(i + 1) * 256].astype(F32)
        squares = squares + part * part
    mean = jnp.sum(squares, axis=1, keepdims=True) * (1.0 / D)
    cols = pl.ds(pl.multiple_of(tp * FEAT, FEAT), FEAT)
    normed = (tok[:, cols].astype(F32) * lax.rsqrt(mean + moe_eps) * mg_in[:, cols]).astype(BF16)
    outgoing = lax.dot_general(
        (pick0 + pick1).astype(BF16), normed, (((0,), (0,)), ((), ())), preferred_element_type=F32
    )
    outbox[...] = outgoing.reshape(N_EP, CAP, FEAT).astype(BF16)

    pl.semaphore_wait(barrier, N_EP - 1 + 3)

    def dispatch(k, carry):
        peer = ep_peer(k)
        rdma(outbox.at[peer], inbox.at[ep], disp_s, disp_r, (peer, tp)).start()
        return carry

    lax.fori_loop(1, N_EP, dispatch, 0)
    inbox[ep] = outbox[ep]

    wd_pair = [rdma(wd_cols(yd, 1 - core), wdx.at[core, yd], wdx_s.at[yd], wdx_r.at[yd], mate) for yd in range(RING)]
    for copy in wd_pair:
        copy.start()
    loads_q.wait()
    q_copies = [
        rdma(qall.at[x], qall.at[x], q_s.at[k - 1], q_r.at[k - 1], (x_peer(k), tp)) for k in range(1, NX)
    ]
    for copy in q_copies:
        copy.start()
    loads_k.wait()
    loads_v.wait()

    def kv_copy(way, d, j):
        origin = ring(z, -(d - 1) if way == 0 else d - 1)
        piece = kv.at[origin, pl.ds(j * KROWS, KROWS)]
        return rdma(piece, piece, kv_s.at[way, d - 1, j], kv_r.at[way, d - 1, j], z_next[way])

    def travels(way, d, j, pieces):
        return d < 4 or (j < pieces // 2) == (way == 0)

    for j in range(KSUB):
        for way in range(2):
            kv_copy(way, 1, j).start()

    def kv_step(d):
        for j in range(KSUB):
            for way in range(2):
                if travels(way, d, j, KSUB):
                    kv_copy(way, d, j).wait_recv()
                    if d < 4 and travels(way, d + 1, j, KSUB):
                        kv_copy(way, d + 1, j).start()

    whole_in = inbox.at[pl.ds(0, N_EP - 1)]
    rdma(whole_in, whole_in, disp_s, disp_r, mate).wait_recv()
    gath[tp] = inbox[...].astype(F32).reshape(SLOTS, FEAT).astype(BF16)

    def gath_piece(origin, c, j):
        return gath.at[origin * 2 + c, pl.ds(j * SROWS, SROWS)]

    def ag_copy(way, d, j):
        origin = ring(y, -(d - 1) if way == 0 else d - 1)
        piece = gath_piece(origin, core, j)
        return rdma(piece, piece, ag_s.at[way, d - 1, j], ag_r.at[way, d - 1, j], y_next[way])

    def dd_copy(rel, j):
        piece = gath_piece(ring(y, rel), core, j)
        return rdma(piece, piece, dd_s.at[rel, j], dd_r.at[rel, j], mate)

    for j in range(SUB):
        for way in range(2):
            ag_copy(way, 1, j).start()
        dd_copy(0, j).start()
    for d in range(1, 5):
        for j in range(SUB):
            for way in range(2):
                if travels(way, d, j, SUB):
                    ag_copy(way, d, j).wait_recv()
                    if d < 4 and travels(way, d + 1, j, SUB):
                        ag_copy(way, d + 1, j).start()
                    dd_copy((RING - d) if way == 0 else d, j).start()
        kv_step(d)
    for rel in range(RING):
        for j in range(SUB):
            dd_copy(rel, j).wait_recv()
    load_wg.wait()
    load_wu.wait()

    acc = jnp.zeros((SLOTS, 2 * FFL), F32)
    for t in range(N_TP):
        acc = acc + jnp.dot(gath[t], wgu[t * FEAT:(t + 1) * FEAT, :], preferred_element_type=F32)
    gate_act, up_act = acc[:, :FFL], acc[:, FFL:]
    hid[core] = (gate_act * jax.nn.sigmoid(gate_act) * up_act).astype(BF16)
    hid_copy = rdma(hid.at[core], hid.at[core], hid_s, hid_r, mate)
    hid_copy.start()
    for yd in range(RING):
        wd_load(yd).wait()
        wd_pair[yd].wait_recv()
    for copy in q_copies:
        copy.wait_recv()
    hid_copy.wait_recv()

    def attend(xq, m):
        qm = qall[xq, :, m * QKD:(m + 1) * QKD]
        keys = kv[:, :, m * QKD:(m + 1) * QKD].reshape(RING * ROWS_A, QKD)
        vals = kv[:, :, 256:512].reshape(RING * ROWS_A, VD)
        s = lax.dot_general(qm, keys, (((1,), (1,)), ((), ())), preferred_element_type=F32) * QKD ** (-0.5)
        col = lax.broadcasted_iota(jnp.int32, s.shape, 1)
        row = lax.broadcasted_iota(jnp.int32, s.shape, 0)
        key_pos = (col >> 7) * (NX * ROWS_A) + x * ROWS_A + (col & 127)
        visible = key_pos <= row + (z * NX + xq) * ROWS_A
        s = jnp.where(visible, s, neg_big)
        top = jnp.max(s, axis=1, keepdims=True)
        w = jnp.where(visible, jnp.exp(s - top), 0.0)
        total = jnp.sum(w, axis=1, keepdims=True)
        o = jnp.dot(w.astype(BF16), vals, preferred_element_type=F32)
        return o, top, total

    def attend_block(k):
        xq = lax.rem(x + k, NX)
        o0, m0, l0 = attend(xq, 0)
        osend[k, :, 0:VD] = o0.astype(BF16)
        o1, m1, l1 = attend(xq, 1)
        osend[k, :, VD:2 * VD] = o1.astype(BF16)
        sl = lax.broadcasted_iota(jnp.int32, (ROWS_A, 128), 1)
        ssend[k] = jnp.where(sl == 0, m0, jnp.where(sl == 1, l0, jnp.where(sl == 2, m1, l1)))

    def o_copies(k):
        dev = (x_peer(k), tp)
        return (
            rdma(osend.at[k], orecv.at[k - 1], o_s.at[0, k - 1], o_r.at[0, k - 1], dev),
            rdma(ssend.at[k], srecv.at[k - 1], o_s.at[1, k - 1], o_r.at[1, k - 1], dev),
        )

    def attend_step(k):
        attend_block(k)
        if k > 0:
            for copy in o_copies(k):
                copy.start()

    hid0, hid1 = hid[0], hid[1]

    def own_term(rel):
        yd = ring(y, rel)
        zown[rel] = jnp.dot(hid0, wdx[0, yd], preferred_element_type=F32) + jnp.dot(
            hid1, wdx[1, yd], preferred_element_type=F32
        )

    def rel_of(way, r):
        return r % RING if way == 0 else (RING - r) % RING

    def rs_copy(way, r, j):
        rows = pl.ds(j * SROWS, SROWS)
        return rdma(
            sbuf.at[way, r - 1, rows], rbuf.at[way, r - 1, rows],
            rsc_s.at[way, r - 1, j], rsc_r.at[way, r - 1, j], y_next[way],
        )

    def rs_send(way, r, j):
        rows = slice(j * SROWS, (j + 1) * SROWS)
        term = zown[rel_of(way, r), rows, :]
        if r < 4 and travels(way, r + 1, j, SUB):
            rs_copy(way, r + 1, j).wait_recv()
            term = term + rbuf[way, r, rows, :].astype(F32)
        sbuf[way, r - 1, rows, :] = term.astype(BF16)
        rs_copy(way, r, j).start()

    own_term(4)
    for j in range(SUB):
        for way in range(2):
            if travels(way, 4, j, SUB):
                rs_send(way, 4, j)
    own_term(3)
    own_term(5)
    order = {0: list(range(SUB // 2, SUB)) + list(range(SUB // 2)), 1: list(range(SUB))}
    for i in range(SUB):
        for way in range(2):
            rs_send(way, 3, order[way][i])
        if i == SUB // 2 - 1:
            for rel in (2, 6, 1, 7, 0):
                own_term(rel)
            attend_step(1)
    attend_step(2)
    for r in (2, 1):
        for i in range(SUB):
            for way in range(2):
                rs_send(way, r, order[way][i])
        attend_step(3 if r == 2 else 0)
    for j in range(SUB):
        rows = slice(j * SROWS, (j + 1) * SROWS)
        rs_copy(0, 1, j).wait_recv()
        rs_copy(1, 1, j).wait_recv()
        result = zown[0, rows, :] + rbuf[0, 0, rows, :].astype(F32) + rbuf[1, 0, rows, :].astype(F32)
        ebox[j * (SROWS // CAP):(j + 1) * (SROWS // CAP)] = result.reshape(SROWS // CAP, CAP, FEAT).astype(BF16)

    def send_back(k, carry):
        peer = ep_peer(k)
        rdma(ebox.at[peer], retbox.at[ep], ret_s, ret_r, (peer, tp)).start()
        return carry

    lax.fori_loop(1, N_EP, send_back, 0)
    retbox[ep] = ebox[ep]

    for k in range(1, NX):
        for copy in o_copies(k):
            copy.wait_recv()

    def joined(m):
        tops = [ssend[0, :, 2 * m:2 * m + 1]] + [srecv[k, :, 2 * m:2 * m + 1] for k in range(NX - 1)]
        sums = [ssend[0, :, 2 * m + 1:2 * m + 2]] + [srecv[k, :, 2 * m + 1:2 * m + 2] for k in range(NX - 1)]
        outs = [osend[0, :, m * VD:(m + 1) * VD]] + [orecv[k, :, m * VD:(m + 1) * VD] for k in range(NX - 1)]
        top = jnp.maximum(jnp.maximum(tops[0], tops[1]), jnp.maximum(tops[2], tops[3]))
        scale = [jnp.exp(t - top) for t in tops]
        total = sum(f * s for f, s in zip(scale, sums))
        return sum(f * o.astype(F32) for f, o in zip(scale, outs)) / total

    mixed = joined(0) - lam_in[...] * joined(1)
    power = jnp.mean(mixed * mixed, axis=1, keepdims=True)
    att_out[...] = (mixed * lax.rsqrt(power + head_eps) * hg_in[...] * head_scale).astype(BF16)

    whole_ret = retbox.at[pl.ds(0, N_EP - 1)]
    rdma(whole_ret, whole_ret, ret_s, ret_r, mate).wait_recv()
    back = retbox[...].astype(F32).reshape(SLOTS, FEAT).astype(BF16)
    first = jnp.dot(pick0.astype(BF16), back, preferred_element_type=F32)
    second = jnp.dot(pick1.astype(BF16), back, preferred_element_type=F32)
    exp_out[...] = (g0 * first + g1 * second).astype(BF16)

    whole_out = outbox.at[pl.ds(0, N_EP - 1)]
    rdma(whole_out, whole_out, disp_s, disp_r, mate).wait_send()
    whole_e = ebox.at[pl.ds(0, N_EP - 1)]
    rdma(whole_e, whole_e, ret_s, ret_r, mate).wait_send()
    for copy in wd_pair + q_copies + [hid_copy]:
        copy.wait_send()
    for k in range(1, NX):
        for copy in o_copies(k):
            copy.wait_send()
    for way in range(2):
        for d in range(1, 5):
            for j in range(KSUB):
                if travels(way, d, j, KSUB):
                    kv_copy(way, d, j).wait_send()
            for j in range(SUB):
                if travels(way, d, j, SUB):
                    ag_copy(way, d, j).wait_send()
                    rs_copy(way, d, j).wait_send()
    for rel in range(RING):
        for j in range(SUB):
            dd_copy(rel, j).wait_send()


def local(
    queries, key_rows, values, lambdas, head_gain, tokens, moe_gain, routes, route_scores, w_gate, w_up, w_down,
):
    hbm = pl.BlockSpec(memory_space=pl.ANY)
    vmem = pl.BlockSpec(memory_space=pltpu.VMEM)
    dma = pltpu.SemaphoreType.DMA
    scratch = [
        pltpu.VMEM((ROWS_B, D), BF16),
        dma((4,)),
        dma((2 + RING,)),
        pltpu.VMEM((N_EP, CAP, FEAT), BF16),
        pltpu.VMEM((N_EP, CAP, FEAT), BF16),
        pltpu.VMEM((N_TP, SLOTS, FEAT), BF16),
        pltpu.VMEM((D, 2 * FFL), BF16),
        pltpu.VMEM((2, RING, FFL, FEAT), BF16),
        pltpu.VMEM((2, SLOTS, FFL), BF16),
        pltpu.VMEM((RING, SLOTS, FEAT), F32),
        pltpu.VMEM((2, 4, SLOTS, FEAT), BF16),
        pltpu.VMEM((2, 4, SLOTS, FEAT), BF16),
        pltpu.VMEM((N_EP, CAP, FEAT), BF16),
        pltpu.VMEM((N_EP, CAP, FEAT), BF16),
        pltpu.VMEM((NX, ROWS_A, 2 * QKD), BF16),
        pltpu.VMEM((RING, ROWS_A, 512), BF16),
        pltpu.VMEM((NX, ROWS_A, 2 * VD), BF16),
        pltpu.VMEM((NX, ROWS_A, 128), F32),
        pltpu.VMEM((NX - 1, ROWS_A, 2 * VD), BF16),
        pltpu.VMEM((NX - 1, ROWS_A, 128), F32),
        dma, dma,
        dma((2, 4, SUB)), dma((2, 4, SUB)),
        dma((RING, SUB)), dma((RING, SUB)),
        dma((RING,)), dma((RING,)),
        dma, dma,
        dma((2, 4, SUB)), dma((2, 4, SUB)),
        dma, dma,
        dma((NX - 1,)), dma((NX - 1,)),
        dma((2, 4, KSUB)), dma((2, 4, KSUB)),
        dma((2, NX - 1)), dma((2, NX - 1)),
    ]
    return pl.pallas_call(
        kernel,
        out_shape=(
            jax.ShapeDtypeStruct((ROWS_A, VD), BF16),
            jax.ShapeDtypeStruct((ROWS_B, FEAT), BF16),
        ),
        in_specs=[hbm, hbm, hbm, vmem, vmem, hbm, vmem, vmem, vmem, hbm, hbm, hbm],
        out_specs=(vmem, vmem),
        scratch_shapes=scratch,
        compiler_params=pltpu.CompilerParams(
            collective_id=0, has_side_effects=True, vmem_limit_bytes=40 * 1024 * 1024
        ),
    )(
        queries, key_rows, values, lambdas.reshape(1, 1), head_gain.reshape(1, VD), tokens,
        moe_gain.reshape(1, D), routes, route_scores, w_gate, w_up, w_down,
    )


def solution(mesh):
    return jax.shard_map(
        local,
        mesh=mesh,
        in_specs=(
            P("ep", "tp"), P("ep", "tp"), P("ep", "tp"), P("tp"), P(), P("ep", None), P(),
            P("ep", None), P("ep", None), P("ep", None, "tp"), P("ep", None, "tp"), P("ep", "tp", None),
        ),
        out_specs=(P("ep", "tp"), P("ep", "tp")),
        check_vma=False,
    )
```

time: 183 us -> 77.3 us (0.42)
  waiting for transfers between devices: 95.5 us -> 0 us
  Pallas kernels: 0 us -> 65.4 us
  starting transfers between devices: 30.2 us -> 0 us
  between operations: 16.2 us -> 1.34 us
  matrix products: 14.6 us -> 0 us
  other arithmetic: 9.36 us -> 0 us
  local copies, waits for them, and re-layouts: 16 us -> 9.91 us
    all_to_all x3 -> x0, waiting for transfers between devices: 95.5 us -> none  [the longest x1 50.9 us: local(): lax.all_to_all(outgoing, 'ep', split_axis=0, concat_axis=0, tiled=True)]
    pallas_call x0 -> x1, Pallas kernels: none -> 65.4 us  [local(): pl.pallas_call(kernel, out_shape=(jax.ShapeDtypeStruct((ROWS_A, VD), BF16...]
    all_to_all x3 -> x0, starting transfers between devices: 30.1 us -> none  [the longest x1 13.8 us: local(): lax.all_to_all(outgoing, 'ep', split_axis=0, concat_axis=0, tiled=True)]
    dot_general x8 -> x0, matrix products: 14.6 us -> none  [the longest x2 5.05 us: fold_block(): accumulated = jnp.einsum('hmqk,khd->hmqd', weights, value_heads)]
    unnamed x19 -> x22, local copies, waits for them, and re-layouts: 1.71 us -> 9.91 us
    reduce_sum x7 -> x0, other arithmetic: 4.59 us -> none  [the longest x2 1.31 us: fold_block(): denominators = jnp.sum(weights, axis=-1)]
    convert_element_type x1 -> x0, local copies, waits for them, and re-layouts: 3.94 us -> none  [local(): value_block.reshape(key_count, head_local, VD).astype(jnp.float32)]
    reshape x2 -> x0, local copies, waits for them, and re-layouts: 3.27 us -> none  [the longest x1 3.13 us: split_up(): return jnp.moveaxis(value.reshape(*before, peers, -1, *after), dim, 0)]
  transfers between devices with their start and end apart: 4 -> 0, of which waited for: 2 -> 0; matrix products, arithmetic and copies ran while one was open for 16% -> 0% of each run, Pallas kernels for 0% -> 0%
where the time goes in v1:
time: 77.3 us; the launch traced here: 76.6 us
  Pallas kernels  65.4 us (85%)
  local copies, waits for them, and re-layouts  9.91 us (13%)
  between operations  1.34 us (2%)
    pallas_call x1, Pallas kernels, local(): pl.pallas_call(kernel, out_shape=(jax.ShapeDtypeStruct((ROWS_A, VD), BF16...  65.4 us
    unnamed x22, local copies, waits for them, and re-layouts  9.91 us

profile of v1, /device:TPU:1, one launch (start us, length us, event | category | flops | bytes accessed | tf_op | source)
XLA Modules:
  0.0 76.6 jit_solution(10485854637151325679)
XLA Ops:
  0.6 0.0 copy-start.4
  1.3 0.8 %copy.14.routes_in = s32[64,2]{1,0:T(8,128)S(1)} copy(s32[64,2]{0,1:T(2,128)} %param.19) | data formatting | bytes 1024 | tf_op args[7]
  2.1 0.0 copy-start.8
  2.1 0.8 %copy.15.rs_in = f32[64,2]{1,0:T(8,128)S(1)} copy(f32[64,2]{0,1:T(2,128)} %param.20) | data formatting | bytes 1024 | tf_op args[8]
  2.9 0.0 copy-done.4
  2.9 0.0 copy-done.8
  2.9 0.0 copy-start
  2.9 1.2 %copy-done = bf16[1,4096,128]{2,1,0:T(8,128)(2,1)S(1)} copy-done((bf16[1,4096,128]{2,1,0:T(8,128)(2,1)S(1)}, bf16[1,4096,128]{2,1,0:T(8,128)(2,1)}, u32[]{:S(2)}) %copy-start) | copy-done | bytes 1048600
  4.1 0.0 copy-start.1
  4.1 1.2 %copy-done.1 = bf16[1,4096,128]{2,1,0:T(8,128)(2,1)S(1)} copy-done((bf16[1,4096,128]{2,1,0:T(8,128)(2,1)S(1)}, bf16[1,4096,128]{2,1,0:T(8,128)(2,1)}, u32[]{:S(2)}) %copy-start.1) | copy-done | bytes 1048600
  5.3 0.0 copy-start.2
  5.3 1.2 %copy-done.2 = bf16[1,128,4096]{2,1,0:T(8,128)(2,1)S(1)} copy-done((bf16[1,128,4096]{2,1,0:T(8,128)(2,1)S(1)}, bf16[1,128,4096]{2,1,0:T(8,128)(2,1)}, u32[]{:S(2)}) %copy-start.2) | copy-done | bytes 1048600
  6.6 0.0 copy-start.3
  6.6 1.0 %copy-done.3 = bf16[64,4096]{1,0:T(8,128)(2,1)S(1)} copy-done((bf16[64,4096]{1,0:T(8,128)(2,1)S(1)}, bf16[64,4096]{1,0:T(8,128)(2,1)}, u32[]{:S(2)}) %copy-start.3) | copy-done | bytes 524312
  7.6 0.0 copy-start.5
  7.6 0.8 %copy-done.5 = bf16[128,256]{1,0:T(8,128)(2,1)S(1)} copy-done((bf16[128,256]{1,0:T(8,128)(2,1)S(1)}, bf16[128,256]{1,0:T(8,128)(2,1)}, u32[]{:S(2)}) %copy-start.5) | copy-done | bytes 65560
  8.4 0.0 copy-start.6
  8.4 0.8 %copy-done.6 = bf16[128,256]{1,0:T(8,128)(2,1)S(1)} copy-done((bf16[128,256]{1,0:T(8,128)(2,1)S(1)}, bf16[128,256]{1,0:T(8,128)(2,1)}, u32[]{:S(2)}) %copy-start.6) | copy-done | bytes 65560
  9.3 0.0 copy-start.7
  9.3 0.7 copy-done.7
  10.0 65.4 %shard_map.131 = (bf16[128,256]{1,0:T(8,128)(2,1)S(1)}, bf16[64,256]{1,0:T(8,128)(2,1)S(1)}) custom-call(bf16[128,256]{1,0:T(8,128)(2,1)S(1)} %copy-done.4, bf16[128,256]{1,0:T(8,128)(2,1)S(1)} %copy-done.5, bf16[128,256]{1,0:T(8,128)(2,1)S(1)} %copy-done.6, f32[1,1]{1,0:T(1,128)} %bitcast.3.lam_in, f32[1,256]{1,0:T(1,128)S(1)} %bitcast.5, ...), custom_call_target="tpu_custom_call" | custom-call | tf_op jit(solution)/shard_map/pallas_call | solution.py:411
  75.4 0.6 copy.19
  76.0 0.6 copy.20
Async XLA Ops:
  0.6 2.2 %copy-start.4 = (bf16[128,256]{1,0:T(8,128)(2,1)S(1)}, bf16[128,256]{1,0:T(8,128)(2,1)}, u32[]{:S(2)}) copy-start(bf16[128,256]{1,0:T(8,128)(2,1)} %q_in.1) | copy-start | bytes 196612
  2.1 0.8 %copy-start.8 = (f32[256]{0:T(256)S(1)}, f32[256]{0:T(256)}, u32[]{:S(2)}) copy-start(f32[256]{0:T(256)} %param.16) | copy-start | bytes 3076
  2.9 1.2 %copy-start = (bf16[1,4096,128]{2,1,0:T(8,128)(2,1)S(1)}, bf16[1,4096,128]{2,1,0:T(8,128)(2,1)}, u32[]{:S(2)}) copy-start(bf16[1,4096,128]{2,1,0:T(8,128)(2,1)} %wg_in.1) | copy-start | bytes 3145732
  4.1 1.2 %copy-start.1 = (bf16[1,4096,128]{2,1,0:T(8,128)(2,1)S(1)}, bf16[1,4096,128]{2,1,0:T(8,128)(2,1)}, u32[]{:S(2)}) copy-start(bf16[1,4096,128]{2,1,0:T(8,128)(2,1)} %wu_in.1) | copy-start | bytes 3145732
  5.3 1.2 %copy-start.2 = (bf16[1,128,4096]{2,1,0:T(8,128)(2,1)S(1)}, bf16[1,128,4096]{2,1,0:T(8,128)(2,1)}, u32[]{:S(2)}) copy-start(bf16[1,128,4096]{2,1,0:T(8,128)(2,1)} %wd_in.1) | copy-start | bytes 3145732
  6.6 1.0 %copy-start.3 = (bf16[64,4096]{1,0:T(8,128)(2,1)S(1)}, bf16[64,4096]{1,0:T(8,128)(2,1)}, u32[]{:S(2)}) copy-start(bf16[64,4096]{1,0:T(8,128)(2,1)} %tok_in.1) | copy-start | bytes 1572868
  7.6 0.8 %copy-start.5 = (bf16[128,256]{1,0:T(8,128)(2,1)S(1)}, bf16[128,256]{1,0:T(8,128)(2,1)}, u32[]{:S(2)}) copy-start(bf16[128,256]{1,0:T(8,128)(2,1)} %k_in.1) | copy-start | bytes 196612
  8.4 0.8 %copy-start.6 = (bf16[128,256]{1,0:T(8,128)(2,1)S(1)}, bf16[128,256]{1,0:T(8,128)(2,1)}, u32[]{:S(2)}) copy-start(bf16[128,256]{1,0:T(8,128)(2,1)} %v_in.1) | copy-start | bytes 196612
  9.3 0.7 copy-start.7

commit v2 on v1

v2 whole, which is shorter than its diff:
```python
import jax
import jax.numpy as jnp
from jax import lax
from jax.experimental import pallas as pl
from jax.experimental.pallas import tpu as pltpu
from jax.sharding import PartitionSpec as P

MESH = pl.DeviceIdType.MESH
F32 = jnp.float32
BF16 = jnp.bfloat16

QKD = 128
VD = 256
D = 4096
N_EP = 32
N_TP = 16
NX = 4
RING = 8
CAP = 8
ROWS_A = 128
ROWS_B = 64
SLOTS = N_EP * CAP
FEAT = D // N_TP
FFL = 128
SUB = 4
SROWS = SLOTS // SUB
GSRC = N_EP // SUB
KSUB = 2
KROWS = ROWS_A // KSUB

neg_big = -1e30
head_eps = 1e-05
moe_eps = 1e-06
head_scale = 0.8


def kernel(
    q_in, k_in, v_in, lam_in, hg_in, tok_in, mg_in, routes_in, rs_in, wg_in, wu_in, wd_in,
    att_out, exp_out,
    tok, lam, mg, hg, routes, scores, pick0, pick1, small_sem, wsem,
    outbox, outfar, inbox, infar, gath, acts, wgu, wdx, hid, zown, sbuf, rbuf,
    ebox, retbox, qall, kv, osend, ssend, orecv, srecv,
    disp_s, disp_r, far_s, far_r, ag_s, ag_r, dd_s, dd_r, wdx_s, wdx_r, hid_s, hid_r,
    rsc_s, rsc_r, ret_s, ret_r, q_s, q_r, kv_s, kv_r, o_s, o_r,
):
    ep = lax.axis_index("ep")
    tp = lax.axis_index("tp")
    z, x = lax.div(ep, NX), lax.rem(ep, NX)
    y, core = lax.div(tp, 2), lax.rem(tp, 2)
    mate = (ep, y * 2 + 1 - core)

    def ring(i, d):
        return lax.rem(i + d + RING, RING)

    y_next = ((ep, ring(y, 1) * 2 + core), (ep, ring(y, -1) * 2 + core))
    z_next = ((ring(z, 1) * NX + x, tp), (ring(z, -1) * NX + x, tp))

    def ep_peer(k):
        return lax.rem(ep + k, N_EP)

    def x_peer(k):
        return z * NX + lax.rem(x + k, NX)

    def rdma(src, dst, ssem, rsem, dev):
        return pltpu.make_async_remote_copy(
            src_ref=src, dst_ref=dst, send_sem=ssem, recv_sem=rsem,
            device_id=dev, device_id_type=MESH,
        )

    def took(ref, sem):
        rdma(ref, ref, sem, sem, mate).wait_recv()

    barrier = pltpu.get_barrier_semaphore()

    def greet(k, carry):
        pl.semaphore_signal(barrier, inc=1, device_id=(ep_peer(k + N_EP // 2), tp), device_id_type=MESH)
        return carry

    lax.fori_loop(0, N_EP // 2, greet, 0)
    lax.fori_loop(N_EP // 2 + 1, N_EP, greet, 0)
    for dev in (*y_next, mate):
        pl.semaphore_signal(barrier, inc=1, device_id=dev, device_id_type=MESH)
    for k in range(NX, 128 // 8):
        srecv[k] = jnp.zeros((8, ROWS_A), F32)

    def load(src, dst, sem):
        copy = pltpu.make_async_copy(src, dst, sem)
        copy.start()
        return copy

    tok_load = load(tok_in, tok, small_sem.at[0])
    loads_routes = load(routes_in, routes, small_sem.at[6])
    loads_mg = load(mg_in, mg, small_sem.at[4])
    loads_q = load(q_in, qall.at[x], small_sem.at[1])
    loads_k = load(k_in, kv.at[z, :, pl.ds(0, 256)], small_sem.at[2])
    loads_v = load(v_in, kv.at[z, :, pl.ds(256, 256)], small_sem.at[3])
    loads_scores = load(rs_in, scores, small_sem.at[7])
    loads_hg = load(hg_in, hg, small_sem.at[5])
    loads_lam = load(lam_in, lam, small_sem.at[8])
    load_wg = load(wg_in.at[0], wgu.at[:, pl.ds(0, FFL)], wsem.at[0])
    load_wu = load(wu_in.at[0], wgu.at[:, pl.ds(FFL, FFL)], wsem.at[1])

    def wd_cols(yd, c):
        return wd_in.at[0, :, pl.ds(pl.multiple_of((yd * 2 + c) * FEAT, FEAT), FEAT)]

    wd_loads = [load(wd_cols(yd, core), wdx.at[core, yd], wsem.at[2 + yd]) for yd in range(RING)]

    loads_routes.wait()
    r0, r1 = routes[0:1, :], routes[1:2, :]
    sub = lax.broadcasted_iota(jnp.int32, (N_EP, ROWS_B), 0)
    hit0, hit1 = sub == r0, sub == r1
    named = jnp.where(hit0 | hit1, 1.0, 0.0).astype(BF16)
    row_i = lax.broadcasted_iota(jnp.int32, (ROWS_B, ROWS_B), 0)
    col_i = lax.broadcasted_iota(jnp.int32, (ROWS_B, ROWS_B), 1)
    earlier = jnp.where(row_i < col_i, 1.0, 0.0).astype(BF16)
    before = jnp.dot(named, earlier, preferred_element_type=F32)
    pos0 = jnp.sum(jnp.where(hit0, before, 0.0), axis=0, keepdims=True)
    pos1 = jnp.sum(jnp.where(hit1, before, 0.0), axis=0, keepdims=True)
    slot0 = r0.astype(F32) * CAP + pos0
    slot1 = r1.astype(F32) * CAP + pos1
    slot_sub = lax.broadcasted_iota(jnp.int32, (SLOTS, ROWS_B), 0).astype(F32)
    pick0[...] = jnp.where(slot_sub == slot0, 1.0, 0.0).astype(BF16)
    pick1[...] = jnp.where(slot_sub == slot1, 1.0, 0.0).astype(BF16)

    tok_load.wait()
    loads_mg.wait()
    squares = jnp.zeros((ROWS_B, 256), F32)
    for i in range(D // 256):
        part = tok[:, i * 256:(i + 1) * 256].astype(F32)
        squares = squares + part * part
    mean = jnp.sum(squares, axis=1, keepdims=True) * (1.0 / D)
    inv = lax.rsqrt(mean + moe_eps)
    picks = pick0[...] + pick1[...]

    def sorted_rows(rel):
        cols = pl.ds(pl.multiple_of((ring(y, rel) * 2 + core) * FEAT, FEAT), FEAT)
        normed = (tok[:, cols].astype(F32) * inv * mg[:, cols]).astype(BF16)
        rows = jnp.dot(picks, normed, preferred_element_type=F32)
        return rows.reshape(N_EP, CAP, FEAT).astype(BF16)

    outbox[...] = sorted_rows(0)
    pl.semaphore_wait(barrier, N_EP - 1 + 3)

    def off_of(source_z, dest_z):
        return lax.rem(lax.div(source_z, 2) - lax.div(dest_z, 2) + SUB, SUB)

    def far_side(off):
        return lax.div(off, 2)

    def dispatch(k, carry):
        peer = ep_peer(k)
        off = off_of(z, lax.div(peer, NX))
        rdma(outbox.at[peer], inbox.at[ep], disp_s, disp_r.at[off], (peer, tp)).start()
        return carry

    lax.fori_loop(1, N_EP, dispatch, 0)
    inbox[ep] = outbox[ep]

    loads_q.wait()
    q_copies = [rdma(qall.at[x], qall.at[x], q_s, q_r.at[k - 1], (x_peer(k), tp)) for k in range(1, NX)]
    for copy in q_copies:
        copy.start()
    for yd in range(RING):
        rdma(wd_cols(yd, 1 - core), wdx.at[core, yd], wdx_s, wdx_r, mate).start()

    for i, rel in enumerate((4, 3, 5)):
        outfar[i] = sorted_rows(rel)

    def dispatch_far(k, carry):
        peer = ep_peer(k)
        off = off_of(z, lax.div(peer, NX))
        rdma(outfar.at[0, peer], infar.at[ep, 0], far_s, far_r.at[off], (peer, tp)).start()
        rdma(outfar.at[1 + far_side(off), peer], infar.at[ep, 1], far_s, far_r.at[off], (peer, tp)).start()
        return carry

    lax.fori_loop(1, N_EP, dispatch_far, 0)
    infar[ep, 0] = outfar[0, ep]
    infar[ep, 1] = outfar[1, ep]

    loads_k.wait()
    loads_v.wait()

    def travels(way, off):
        return (off < 2) == (way == 0)

    def kv_moves(way, d, j):
        return d < 4 or (j < KSUB // 2) == (way == 0)

    def kv_copy(way, d, j):
        origin = ring(z, -(d - 1) if way == 0 else d - 1)
        piece = kv.at[origin, pl.ds(j * KROWS, KROWS)]
        return rdma(piece, piece, kv_s, kv_r.at[way, d - 1, j], z_next[way])

    for j in range(KSUB):
        for way in range(2):
            kv_copy(way, 1, j).start()

    def kv_step(d):
        for j in range(KSUB):
            for way in range(2):
                if kv_moves(way, d, j):
                    kv_copy(way, d, j).wait_recv()
                    if d < 4 and kv_moves(way, d + 1, j):
                        kv_copy(way, d + 1, j).start()

    ORDER = (0, 3, 1, 2)

    def rows_of(off):
        return pl.ds(off * SROWS, SROWS)

    def group(off):
        return lax.rem(lax.div(z, 2) + off, SUB) * GSRC

    def gath_piece(rel, off):
        return gath.at[ring(y, rel) * 2 + core, rows_of(off)]

    def ag_copy(way, d, off):
        piece = gath_piece(-(d - 1) if way == 0 else d - 1, off)
        return rdma(piece, piece, ag_s, ag_r.at[way, d - 1, off], y_next[way])

    def to_mate(rel, off, stage):
        piece = gath_piece(rel, off)
        rdma(piece, piece, dd_s, dd_r.at[stage], mate).start()

    def flat(rows):
        return rows.astype(F32).reshape(SROWS, FEAT).astype(BF16)

    for off in ORDER:
        took(inbox.at[pl.ds(0, GSRC - 1 if off == 0 else GSRC)], disp_r.at[off])
        gath[tp, off * SROWS:(off + 1) * SROWS, :] = flat(inbox[pl.ds(group(off), GSRC)])
        for way in range(2):
            ag_copy(way, 1, off).start()
        to_mate(0, off, 0)

    def ag_step(d, off):
        for way in range(2):
            if d < 3 or travels(way, off):
                ag_copy(way, d, off).wait_recv()
                if d == 1 or (d == 2 and travels(way, off)):
                    ag_copy(way, d + 1, off).start()
                to_mate(-d if way == 0 else d, off, d - 1 if d < 3 else 2 + off)

    for off in ORDER:
        ag_step(1, off)
    for off in ORDER:
        ag_step(2, off)
    load_wg.wait()
    load_wu.wait()

    def product(rel, rows):
        terms = []
        for c in range(2):
            t = ring(y, rel) * 2 + c
            weights = wgu[pl.ds(pl.multiple_of(t * FEAT, FEAT), FEAT), :]
            terms.append(jnp.dot(gath[t, rows, :], weights, preferred_element_type=F32))
        return terms[0] + terms[1]

    every = slice(0, SLOTS)
    took(gath.at[pl.ds(0, 3)], dd_r.at[0])
    acts[...] = product(0, every) + product(1, every) + product(-1, every)
    for off in ORDER:
        took(infar.at[pl.ds(0, GSRC - 1 if off == 0 else GSRC)], far_r.at[off])
        sources = pl.ds(group(off), GSRC)
        for i, rel in ((0, 4), (1, 3 if off < 2 else -3)):
            gath[ring(y, rel) * 2 + core, off * SROWS:(off + 1) * SROWS, :] = flat(infar[sources, i])
            to_mate(rel, off, 1)
    kv_step(1)
    took(gath.at[pl.ds(0, 4)], dd_r.at[1])
    acts[...] += product(2, every) + product(-2, every) + product(4, every)
    lower, upper = slice(0, SLOTS // 2), slice(SLOTS // 2, SLOTS)
    acts[lower, :] += product(3, lower)
    acts[upper, :] += product(-3, upper)

    def hid_copy(off):
        piece = hid.at[core, rows_of(off)]
        return rdma(piece, piece, hid_s, hid_r.at[off], mate)

    def expert(off):
        took(gath.at[0, rows_of(off)], dd_r.at[2 + off])
        rows = slice(off * SROWS, (off + 1) * SROWS)
        acc = acts[rows, :] + product(-3 if off < 2 else 3, rows)
        gate_act, up_act = acc[:, :FFL], acc[:, FFL:]
        hid[core, rows, :] = (gate_act * jax.nn.sigmoid(gate_act) * up_act).astype(BF16)
        hid_copy(off).start()

    def rel_of(way, r):
        return r % RING if way == 0 else (RING - r) % RING

    def rs_copy(way, r, off):
        return rdma(
            sbuf.at[way, r - 1, rows_of(off)], rbuf.at[way, r - 1, rows_of(off)],
            rsc_s, rsc_r.at[way, r - 1, off], y_next[way],
        )

    def rs_send(way, r, off):
        rows = slice(off * SROWS, (off + 1) * SROWS)
        term = zown[rel_of(way, r), rows, :]
        if r < 3 or (r == 3 and travels(way, off)):
            rs_copy(way, r + 1, off).wait_recv()
            term = term + rbuf[way, r, rows, :].astype(F32)
        sbuf[way, r - 1, rows, :] = term.astype(BF16)
        rs_copy(way, r, off).start()

    def own_terms(rows, rels):
        hid0, hid1 = hid[0, rows, :], hid[1, rows, :]
        for rel in rels:
            yd = ring(y, rel)
            zown[rel, rows, :] = jnp.dot(hid0, wdx[0, yd], preferred_element_type=F32) + jnp.dot(
                hid1, wdx[1, yd], preferred_element_type=F32
            )

    def launch(off):
        hid_copy(off).wait_recv()
        long_way = 0 if off < 2 else 1
        own_terms(slice(off * SROWS, (off + 1) * SROWS), (4, 3, 5))
        rs_send(long_way, 4, off)
        rs_send(1 - long_way, 3, off)

    ag_step(3, ORDER[0])
    ag_step(3, ORDER[1])
    expert(ORDER[0])
    ag_step(3, ORDER[2])
    expert(ORDER[1])
    for copy in wd_loads:
        copy.wait()
    took(wdx.at[0], wdx_r)
    ag_step(3, ORDER[3])
    launch(ORDER[0])
    expert(ORDER[2])
    launch(ORDER[1])
    expert(ORDER[3])
    launch(ORDER[2])
    kv_step(2)
    launch(ORDER[3])
    own_terms(every, (2, 6))

    def attend(xq, m):
        qm = qall[xq, :, m * QKD:(m + 1) * QKD]
        keys = kv[:, :, m * QKD:(m + 1) * QKD].reshape(RING * ROWS_A, QKD)
        vals = kv[:, :, 256:512].reshape(RING * ROWS_A, VD)
        s = lax.dot_general(qm, keys, (((1,), (1,)), ((), ())), preferred_element_type=F32) * QKD ** (-0.5)
        col = lax.broadcasted_iota(jnp.int32, s.shape, 1)
        row = lax.broadcasted_iota(jnp.int32, s.shape, 0)
        key_pos = (col >> 7) * (NX * ROWS_A) + x * ROWS_A + (col & 127)
        visible = key_pos <= row + (z * NX + xq) * ROWS_A
        s = jnp.where(visible, s, neg_big)
        top = jnp.max(s, axis=1, keepdims=True)
        w = jnp.where(visible, jnp.exp(s - top), 0.0)
        total = jnp.sum(w, axis=1, keepdims=True)
        o = jnp.dot(w.astype(BF16), vals, preferred_element_type=F32)
        return o, top, total

    def attend_block(k):
        xq = lax.rem(x + k, NX)
        o0, m0, l0 = attend(xq, 0)
        osend[k, :, 0:VD] = o0.astype(BF16)
        o1, m1, l1 = attend(xq, 1)
        osend[k, :, VD:2 * VD] = o1.astype(BF16)
        sl = lax.broadcasted_iota(jnp.int32, (ROWS_A, 128), 1)
        stats = jnp.where(sl == 0, m0, jnp.where(sl == 1, l0, jnp.where(sl == 2, m1, l1)))
        ssend[k] = stats.T[0:8, :]

    def o_copies(k):
        dev = (x_peer(k), tp)
        return (
            rdma(osend.at[k], orecv.at[k - 1], o_s.at[0], o_r.at[0, k - 1], dev),
            rdma(ssend.at[k], srecv.at[k], o_s.at[1], o_r.at[1, k - 1], dev),
        )

    def attend_step(k):
        attend_block(k)
        if k > 0:
            for copy in o_copies(k):
                copy.start()

    for off in ORDER:
        rs_send(0 if off < 2 else 1, 3, off)
    own_terms(every, (1, 7, 0))
    kv_step(3)
    LATER = (3, 1, 2, 0)
    for off in LATER:
        for way in range(2):
            rs_send(way, 2, off)
    kv_step(4)
    for copy in q_copies:
        copy.wait_recv()
    attend_step(2)
    for off in LATER[:2]:
        for way in range(2):
            rs_send(way, 1, off)
    attend_step(1)
    for off in LATER[2:]:
        for way in range(2):
            rs_send(way, 1, off)
    attend_step(3)

    for off in LATER:
        rows = slice(off * SROWS, (off + 1) * SROWS)
        rs_copy(0, 1, off).wait_recv()
        rs_copy(1, 1, off).wait_recv()
        result = zown[0, rows, :] + rbuf[0, 0, rows, :].astype(F32) + rbuf[1, 0, rows, :].astype(F32)
        ebox[off * GSRC:(off + 1) * GSRC] = result.reshape(GSRC, CAP, FEAT).astype(BF16)
        first = group(off)
        for i in range(GSRC):
            peer = first + i
            if off > 0:
                rdma(ebox.at[off * GSRC + i], retbox.at[ep], ret_s, ret_r, (peer, tp)).start()
            else:

                @pl.when(peer != ep)
                def _():
                    rdma(ebox.at[off * GSRC + i], retbox.at[ep], ret_s, ret_r, (peer, tp)).start()

    retbox[ep] = ebox[lax.rem(ep, GSRC)]
    attend_step(0)

    for k in range(1, NX):
        for copy in o_copies(k):
            copy.wait_recv()

    srecv[0] = ssend[0]
    stats = srecv[...].reshape(128, ROWS_A).T

    def joined(m):
        tops = [stats[:, 8 * k + 2 * m:8 * k + 2 * m + 1] for k in range(NX)]
        sums = [stats[:, 8 * k + 2 * m + 1:8 * k + 2 * m + 2] for k in range(NX)]
        outs = [osend[0, :, m * VD:(m + 1) * VD]] + [orecv[k, :, m * VD:(m + 1) * VD] for k in range(NX - 1)]
        top = jnp.maximum(jnp.maximum(tops[0], tops[1]), jnp.maximum(tops[2], tops[3]))
        scale = [jnp.exp(t - top) for t in tops]
        total = sum(f * s for f, s in zip(scale, sums))
        return sum(f * o.astype(F32) for f, o in zip(scale, outs)) / total

    loads_hg.wait()
    loads_lam.wait()
    mixed = joined(0) - lam[0] * joined(1)
    power = jnp.mean(mixed * mixed, axis=1, keepdims=True)
    att_out[...] = (mixed * lax.rsqrt(power + head_eps) * hg[...] * head_scale).astype(BF16)
    loads_scores.wait()
    s0, s1 = scores[0:1, :], scores[1:2, :]
    smax = jnp.maximum(s0, s1)
    e0, e1 = jnp.exp(s0 - smax), jnp.exp(s1 - smax)
    esum = e0 + e1
    same = row_i == col_i
    g0 = jnp.sum(jnp.where(same, e0 / esum, 0.0), axis=1, keepdims=True)
    g1 = jnp.sum(jnp.where(same, e1 / esum, 0.0), axis=1, keepdims=True)

    took(inbox.at[pl.ds(0, N_EP - 1)], disp_s)
    took(infar.at[pl.ds(0, N_EP - 1)], far_s)
    took(qall.at[pl.ds(0, NX - 1)], q_s)
    took(wdx.at[0], wdx_s)
    took(hid.at[0], hid_s)
    took(gath.at[pl.ds(0, 5)], ag_s)
    took(gath.at[pl.ds(0, RING)], dd_s)
    took(gath.at[pl.ds(0, 7)], rsc_s)
    took(gath.at[pl.ds(0, 7)], kv_s)
    took(osend.at[pl.ds(0, NX - 1)], o_s.at[0])
    took(ssend.at[pl.ds(0, NX - 1)], o_s.at[1])
    took(ebox.at[pl.ds(0, N_EP - 1)], ret_s)

    took(retbox.at[pl.ds(0, N_EP - 1)], ret_r)
    back = retbox[...].astype(F32).reshape(SLOTS, FEAT).astype(BF16)
    contract = (((0,), (0,)), ((), ()))
    first = lax.dot_general(pick0[...], back, contract, preferred_element_type=F32)
    second = lax.dot_general(pick1[...], back, contract, preferred_element_type=F32)
    exp_out[...] = (g0 * first + g1 * second).astype(BF16)


def local(
    queries, key_rows, values, lambdas, head_gain, tokens, moe_gain, routes, route_scores, w_gate, w_up, w_down,
):
    hbm = pl.BlockSpec(memory_space=pltpu.HBM)
    vmem = pl.BlockSpec(memory_space=pltpu.VMEM)
    dma = pltpu.SemaphoreType.DMA
    boxes = (N_EP, CAP, FEAT)
    scratch = [
        pltpu.VMEM((ROWS_B, D), BF16),
        pltpu.SMEM((1,), F32),
        pltpu.VMEM((1, D), F32),
        pltpu.VMEM((1, VD), F32),
        pltpu.VMEM((2, ROWS_B), jnp.int32),
        pltpu.VMEM((2, ROWS_B), F32),
        pltpu.VMEM((SLOTS, ROWS_B), BF16),
        pltpu.VMEM((SLOTS, ROWS_B), BF16),
        dma((9,)),
        dma((2 + RING,)),
        pltpu.VMEM(boxes, BF16),
        pltpu.VMEM((3, *boxes), BF16),
        pltpu.VMEM(boxes, BF16),
        pltpu.VMEM((N_EP, 2, CAP, FEAT), BF16),
        pltpu.VMEM((N_TP, SLOTS, FEAT), BF16),
        pltpu.VMEM((SLOTS, 2 * FFL), F32),
        pltpu.VMEM((D, 2 * FFL), BF16),
        pltpu.VMEM((2, RING, FFL, FEAT), BF16),
        pltpu.VMEM((2, SLOTS, FFL), BF16),
        pltpu.VMEM((RING, SLOTS, FEAT), F32),
        pltpu.VMEM((2, 4, SLOTS, FEAT), BF16),
        pltpu.VMEM((2, 4, SLOTS, FEAT), BF16),
        pltpu.VMEM(boxes, BF16),
        pltpu.VMEM(boxes, BF16),
        pltpu.VMEM((NX, ROWS_A, 2 * QKD), BF16),
        pltpu.VMEM((RING, ROWS_A, 512), BF16),
        pltpu.VMEM((NX, ROWS_A, 2 * VD), BF16),
        pltpu.VMEM((NX, 8, ROWS_A), F32),
        pltpu.VMEM((NX - 1, ROWS_A, 2 * VD), BF16),
        pltpu.VMEM((128 // 8, 8, ROWS_A), F32),
        dma, dma((SUB,)),
        dma, dma((SUB,)),
        dma, dma((2, 3, SUB)),
        dma, dma((2 + SUB,)),
        dma, dma,
        dma, dma((SUB,)),
        dma, dma((2, 4, SUB)),
        dma, dma,
        dma, dma((NX - 1,)),
        dma, dma((2, 4, KSUB)),
        dma((2,)), dma((2, NX - 1)),
    ]
    return pl.pallas_call(
        kernel,
        out_shape=(
            pltpu.VMEM((ROWS_A, VD), BF16),
            pltpu.VMEM((ROWS_B, FEAT), BF16),
        ),
        in_specs=[hbm, hbm, hbm, hbm, hbm, hbm, hbm, hbm, hbm, hbm, hbm, hbm],
        out_specs=(vmem, vmem),
        scratch_shapes=scratch,
        compiler_params=pltpu.CompilerParams(
            collective_id=0, has_side_effects=True, vmem_limit_bytes=63000000
        ),
    )(
        queries, key_rows, values, lambdas, head_gain.reshape(1, VD), tokens,
        moe_gain.reshape(1, D), routes.T, route_scores.T, w_gate, w_up, w_down,
    )


def solution(mesh):
    return jax.shard_map(
        local,
        mesh=mesh,
        in_specs=(
            P("ep", "tp"), P("ep", "tp"), P("ep", "tp"), P("tp"), P(), P("ep", None), P(),
            P("ep", None), P("ep", None), P("ep", None, "tp"), P("ep", None, "tp"), P("ep", "tp", None),
        ),
        out_specs=(P("ep", "tp"), P("ep", "tp")),
        check_vma=False,
    )
```

time: 77.3 us -> 60.3 us (0.78)
  the two profiles are of different devices: /device:TPU:1 before, /device:TPU:16 now
where the time goes in v2:
time: 60.3 us; the launch traced here: 60.1 us
  Pallas kernels  57.6 us (96%)
  between operations  1.29 us (2%)
  local copies, waits for them, and re-layouts  1.25 us (2%)
    pallas_call x1, Pallas kernels, local(): pl.pallas_call(kernel, out_shape=(pltpu.VMEM((ROWS_A, VD), BF16), pltpu.V...  57.6 us
    unnamed x2, local copies, waits for them, and re-layouts  1.25 us

profile of v2, /device:TPU:16, one launch (start us, length us, event | category | flops | bytes accessed | tf_op | source)
XLA Modules:
  0.0 60.1 jit_solution(12541931961963559053)
XLA Ops:
  1.3 57.6 %shard_map.131 = (bf16[128,256]{1,0:T(8,128)(2,1)S(1)}, bf16[64,256]{1,0:T(8,128)(2,1)S(1)}) custom-call(bf16[128,256]{1,0:T(8,128)(2,1)} %q_in.1, bf16[128,256]{1,0:T(8,128)(2,1)} %k_in.1, bf16[128,256]{1,0:T(8,128)(2,1)} %v_in.1, f32[1]{0:T(128)S(6)} %copy.18.lam_in, f32[1,256]{1,0:T(1,128)} %bitcast.5, bf16[64,4096]{1,0:T(8,128)(2,1)} %tok_in.1, ...), custom_call_target="tpu_custom_call" | custom-call | tf_op jit(solution)/shard_map/pallas_call | solution.py:518
  58.9 0.6 %copy.16 = bf16[128,256]{1,0:T(8,128)(2,1)} copy(bf16[128,256]{1,0:T(8,128)(2,1)S(1)} %get-tuple-element.2) | data formatting | bytes 131072
  59.5 0.6 %copy.17 = bf16[64,256]{1,0:T(8,128)(2,1)} copy(bf16[64,256]{1,0:T(8,128)(2,1)S(1)} %get-tuple-element.3) | data formatting | bytes 65536

commit v3 on v2

--- a/solution.py
+++ b/solution.py
@@ -141,41 +141,17 @@
     outbox[...] = sorted_rows(0)
     pl.semaphore_wait(barrier, N_EP - 1 + 3)
 
-    def off_of(source_z, dest_z):
-        return lax.rem(lax.div(source_z, 2) - lax.div(dest_z, 2) + SUB, SUB)
-
-    def far_side(off):
-        return lax.div(off, 2)
+    my_group = lax.div(z, 2)
+    my_side = lax.rem(my_group, 2)
+    my_off = my_side * 2 + lax.div(my_group, 2)
 
     def dispatch(k, carry):
         peer = ep_peer(k)
-        off = off_of(z, lax.div(peer, NX))
-        rdma(outbox.at[peer], inbox.at[ep], disp_s, disp_r.at[off], (peer, tp)).start()
+        rdma(outbox.at[peer], inbox.at[ep], disp_s, disp_r.at[my_off], (peer, tp)).start()
         return carry
 
     lax.fori_loop(1, N_EP, dispatch, 0)
     inbox[ep] = outbox[ep]
-
-    loads_q.wait()
-    q_copies = [rdma(qall.at[x], qall.at[x], q_s, q_r.at[k - 1], (x_peer(k), tp)) for k in range(1, NX)]
-    for copy in q_copies:
-        copy.start()
-    for yd in range(RING):
-        rdma(wd_cols(yd, 1 - core), wdx.at[core, yd], wdx_s, wdx_r, mate).start()
-
-    for i, rel in enumerate((4, 3, 5)):
-        outfar[i] = sorted_rows(rel)
-
-    def dispatch_far(k, carry):
-        peer = ep_peer(k)
-        off = off_of(z, lax.div(peer, NX))
-        rdma(outfar.at[0, peer], infar.at[ep, 0], far_s, far_r.at[off], (peer, tp)).start()
-        rdma(outfar.at[1 + far_side(off), peer], infar.at[ep, 1], far_s, far_r.at[off], (peer, tp)).start()
-        return carry
-
-    lax.fori_loop(1, N_EP, dispatch_far, 0)
-    infar[ep, 0] = outfar[0, ep]
-    infar[ep, 1] = outfar[1, ep]
 
     loads_k.wait()
     loads_v.wait()
@@ -194,6 +170,19 @@
     for j in range(KSUB):
         for way in range(2):
             kv_copy(way, 1, j).start()
+
+    for i, rel in enumerate((4, 3, 5)):
+        outfar[i] = sorted_rows(rel)
+
+    def dispatch_far(k, carry):
+        peer = ep_peer(k)
+        rdma(outfar.at[0, peer], infar.at[ep, 0], far_s, far_r.at[my_off], (peer, tp)).start()
+        rdma(outfar.at[1 + my_side, peer], infar.at[ep, 1], far_s, far_r.at[my_off], (peer, tp)).start()
+        return carry
+
+    lax.fori_loop(1, N_EP, dispatch_far, 0)
+    infar[ep, 0] = outfar[0, ep]
+    infar[ep, 1] = outfar[1 + my_side, ep]
 
     def kv_step(d):
         for j in range(KSUB):
@@ -203,13 +192,23 @@
                     if d < 4 and kv_moves(way, d + 1, j):
                         kv_copy(way, d + 1, j).start()
 
-    ORDER = (0, 3, 1, 2)
+    ORDER = (0, 2, 1, 3)
+    GROUPS = (0, 2, 1, 3)
 
     def rows_of(off):
         return pl.ds(off * SROWS, SROWS)
 
     def group(off):
-        return lax.rem(lax.div(z, 2) + off, SUB) * GSRC
+        return GROUPS[off] * GSRC
+
+    def arrived(box, sem, off):
+        @pl.when(my_off == off)
+        def _():
+            took(box.at[pl.ds(0, GSRC - 1)], sem.at[off])
+
+        @pl.when(my_off != off)
+        def _():
+            took(box.at[pl.ds(0, GSRC)], sem.at[off])
 
     def gath_piece(rel, off):
         return gath.at[ring(y, rel) * 2 + core, rows_of(off)]
@@ -226,7 +225,7 @@
         return rows.astype(F32).reshape(SROWS, FEAT).astype(BF16)
 
     for off in ORDER:
-        took(inbox.at[pl.ds(0, GSRC - 1 if off == 0 else GSRC)], disp_r.at[off])
+        arrived(inbox, disp_r, off)
         gath[tp, off * SROWS:(off + 1) * SROWS, :] = flat(inbox[pl.ds(group(off), GSRC)])
         for way in range(2):
             ag_copy(way, 1, off).start()
@@ -242,6 +241,13 @@
 
     for off in ORDER:
         ag_step(1, off)
+    kv_step(1)
+    loads_q.wait()
+    q_copies = [rdma(qall.at[x], qall.at[x], q_s, q_r.at[k - 1], (x_peer(k), tp)) for k in range(1, NX)]
+    for copy in q_copies:
+        copy.start()
+    for yd in range(RING):
+        rdma(wd_cols(yd, 1 - core), wdx.at[core, yd], wdx_s, wdx_r, mate).start()
     for off in ORDER:
         ag_step(2, off)
     load_wg.wait()
@@ -259,17 +265,17 @@
     took(gath.at[pl.ds(0, 3)], dd_r.at[0])
     acts[...] = product(0, every) + product(1, every) + product(-1, every)
     for off in ORDER:
-        took(infar.at[pl.ds(0, GSRC - 1 if off == 0 else GSRC)], far_r.at[off])
+        arrived(infar, far_r, off)
         sources = pl.ds(group(off), GSRC)
         for i, rel in ((0, 4), (1, 3 if off < 2 else -3)):
             gath[ring(y, rel) * 2 + core, off * SROWS:(off + 1) * SROWS, :] = flat(infar[sources, i])
             to_mate(rel, off, 1)
-    kv_step(1)
     took(gath.at[pl.ds(0, 4)], dd_r.at[1])
     acts[...] += product(2, every) + product(-2, every) + product(4, every)
     lower, upper = slice(0, SLOTS // 2), slice(SLOTS // 2, SLOTS)
     acts[lower, :] += product(3, lower)
     acts[upper, :] += product(-3, upper)
+    kv_step(2)
 
     def hid_copy(off):
         piece = hid.at[core, rows_of(off)]
@@ -330,35 +336,40 @@
     launch(ORDER[1])
     expert(ORDER[3])
     launch(ORDER[2])
-    kv_step(2)
     launch(ORDER[3])
+    kv_step(3)
     own_terms(every, (2, 6))
 
-    def attend(xq, m):
-        qm = qall[xq, :, m * QKD:(m + 1) * QKD]
-        keys = kv[:, :, m * QKD:(m + 1) * QKD].reshape(RING * ROWS_A, QKD)
-        vals = kv[:, :, 256:512].reshape(RING * ROWS_A, VD)
-        s = lax.dot_general(qm, keys, (((1,), (1,)), ((), ())), preferred_element_type=F32) * QKD ** (-0.5)
-        col = lax.broadcasted_iota(jnp.int32, s.shape, 1)
-        row = lax.broadcasted_iota(jnp.int32, s.shape, 0)
-        key_pos = (col >> 7) * (NX * ROWS_A) + x * ROWS_A + (col & 127)
-        visible = key_pos <= row + (z * NX + xq) * ROWS_A
-        s = jnp.where(visible, s, neg_big)
-        top = jnp.max(s, axis=1, keepdims=True)
-        w = jnp.where(visible, jnp.exp(s - top), 0.0)
-        total = jnp.sum(w, axis=1, keepdims=True)
-        o = jnp.dot(w.astype(BF16), vals, preferred_element_type=F32)
-        return o, top, total
-
-    def attend_block(k):
+    def attend(k, blocks):
         xq = lax.rem(x + k, NX)
-        o0, m0, l0 = attend(xq, 0)
-        osend[k, :, 0:VD] = o0.astype(BF16)
-        o1, m1, l1 = attend(xq, 1)
-        osend[k, :, VD:2 * VD] = o1.astype(BF16)
+        vals = kv[0:blocks, :, 256:512].reshape(blocks * ROWS_A, VD)
+        col = lax.broadcasted_iota(jnp.int32, (ROWS_A, blocks * ROWS_A), 1)
+        row = lax.broadcasted_iota(jnp.int32, (ROWS_A, blocks * ROWS_A), 0)
+        key_pos = (col >> 7) * (NX * ROWS_A) + (col & 127)
+        visible = key_pos - row <= (z * NX + xq - x) * ROWS_A
+        stats = []
+        for m in range(2):
+            qm = qall[xq, :, m * QKD:(m + 1) * QKD]
+            keys = kv[0:blocks, :, m * QKD:(m + 1) * QKD].reshape(blocks * ROWS_A, QKD)
+            s = lax.dot_general(qm, keys, (((1,), (1,)), ((), ())), preferred_element_type=F32) * QKD ** (-0.5)
+            s = jnp.where(visible, s, neg_big)
+            top = jnp.max(s, axis=1, keepdims=True)
+            w = jnp.exp(s - top)
+            stats += [top, jnp.sum(w, axis=1, keepdims=True)]
+            o = jnp.dot(w.astype(BF16), vals, preferred_element_type=F32)
+            osend[k, :, m * VD:(m + 1) * VD] = o.astype(BF16)
         sl = lax.broadcasted_iota(jnp.int32, (ROWS_A, 128), 1)
-        stats = jnp.where(sl == 0, m0, jnp.where(sl == 1, l0, jnp.where(sl == 2, m1, l1)))
-        ssend[k] = stats.T[0:8, :]
+        packed = jnp.where(sl == 0, stats[0], jnp.where(sl == 1, stats[1], jnp.where(sl == 2, stats[2], stats[3])))
+        ssend[k] = packed.T[0:8, :]
+
+    def attend_both(k):
+        @pl.when(z < RING // 2)
+        def _():
+            attend(k, RING // 2)
+
+        @pl.when(z >= RING // 2)
+        def _():
+            attend(k, RING)
 
     def o_copies(k):
         dev = (x_peer(k), tp)
@@ -367,34 +378,36 @@
             rdma(ssend.at[k], srecv.at[k], o_s.at[1], o_r.at[1, k - 1], dev),
         )
 
-    def attend_step(k):
-        attend_block(k)
-        if k > 0:
-            for copy in o_copies(k):
-                copy.start()
-
-    for off in ORDER:
+    def send_half(k):
+        for copy in o_copies(k):
+            copy.start()
+
+    def attend_for(k):
+        attend_both(k)
+        send_half(k)
+
+    for off in ORDER[:2]:
         rs_send(0 if off < 2 else 1, 3, off)
     own_terms(every, (1, 7, 0))
-    kv_step(3)
-    LATER = (3, 1, 2, 0)
-    for off in LATER:
+    for off in ORDER[2:]:
+        rs_send(0 if off < 2 else 1, 3, off)
+    for i, off in enumerate(ORDER):
         for way in range(2):
             rs_send(way, 2, off)
-    kv_step(4)
-    for copy in q_copies:
-        copy.wait_recv()
-    attend_step(2)
-    for off in LATER[:2]:
+        if i == 2:
+            kv_step(4)
+            for copy in q_copies:
+                copy.wait_recv()
+            attend_for(2)
+    for i, off in enumerate(ORDER):
         for way in range(2):
             rs_send(way, 1, off)
-    attend_step(1)
-    for off in LATER[2:]:
-        for way in range(2):
-            rs_send(way, 1, off)
-    attend_step(3)
-
-    for off in LATER:
+        if i == 0:
+            attend_for(1)
+        if i == 2:
+            attend_for(3)
+
+    for off in ORDER:
         rows = slice(off * SROWS, (off + 1) * SROWS)
         rs_copy(0, 1, off).wait_recv()
         rs_copy(1, 1, off).wait_recv()
@@ -403,16 +416,13 @@
         first = group(off)
         for i in range(GSRC):
             peer = first + i
-            if off > 0:
+
+            @pl.when(peer != ep)
+            def _():
                 rdma(ebox.at[off * GSRC + i], retbox.at[ep], ret_s, ret_r, (peer, tp)).start()
-            else:
-
-                @pl.when(peer != ep)
-                def _():
-                    rdma(ebox.at[off * GSRC + i], retbox.at[ep], ret_s, ret_r, (peer, tp)).start()
-
-    retbox[ep] = ebox[lax.rem(ep, GSRC)]
-    attend_step(0)
+
+    retbox[ep] = ebox[my_off * GSRC + lax.rem(ep, GSRC)]
+    attend_both(0)
 
     for k in range(1, NX):
         for copy in o_copies(k):

time: 60.3 us -> 58.3 us (0.967)
  the two profiles are of different devices: /device:TPU:16 before, /device:TPU:1 now
where the time goes in v3:
time: 58.3 us; the launch traced here: 57.3 us
  Pallas kernels  54.8 us (94%)
  between operations  1.29 us (2%)
  local copies, waits for them, and re-layouts  1.25 us (2%)
    pallas_call x1, Pallas kernels, local(): pl.pallas_call(kernel, out_shape=(pltpu.VMEM((ROWS_A, VD), BF16), pltpu.V...  54.8 us
    unnamed x2, local copies, waits for them, and re-layouts  1.25 us

profile of v3, /device:TPU:1, one launch (start us, length us, event | category | flops | bytes accessed | tf_op | source)
XLA Modules:
  0.0 57.3 jit_solution(8482929655330980529)
XLA Ops:
  1.3 54.8 %shard_map.131 = (bf16[128,256]{1,0:T(8,128)(2,1)S(1)}, bf16[64,256]{1,0:T(8,128)(2,1)S(1)}) custom-call(bf16[128,256]{1,0:T(8,128)(2,1)} %q_in.1, bf16[128,256]{1,0:T(8,128)(2,1)} %k_in.1, bf16[128,256]{1,0:T(8,128)(2,1)} %v_in.1, f32[1]{0:T(128)S(6)} %copy.18.lam_in, f32[1,256]{1,0:T(1,128)} %bitcast.5, bf16[64,4096]{1,0:T(8,128)(2,1)} %tok_in.1, ...), custom_call_target="tpu_custom_call" | custom-call | tf_op jit(solution)/shard_map/pallas_call | solution.py:528
  56.1 0.6 %copy.16 = bf16[128,256]{1,0:T(8,128)(2,1)} copy(bf16[128,256]{1,0:T(8,128)(2,1)S(1)} %get-tuple-element.2) | data formatting | bytes 131072
  56.7 0.6 %copy.17 = bf16[64,256]{1,0:T(8,128)(2,1)} copy(bf16[64,256]{1,0:T(8,128)(2,1)S(1)} %get-tuple-element.3) | data formatting | bytes 65536

commit v4 on v3

--- a/solution.py
+++ b/solution.py
@@ -72,12 +72,8 @@
 
     barrier = pltpu.get_barrier_semaphore()
 
-    def greet(k, carry):
-        pl.semaphore_signal(barrier, inc=1, device_id=(ep_peer(k + N_EP // 2), tp), device_id_type=MESH)
-        return carry
-
-    lax.fori_loop(0, N_EP // 2, greet, 0)
-    lax.fori_loop(N_EP // 2 + 1, N_EP, greet, 0)
+    for k in [*range(N_EP // 2, N_EP), *range(1, N_EP // 2)]:
+        pl.semaphore_signal(barrier, inc=1, device_id=(ep_peer(k), tp), device_id_type=MESH)
     for dev in (*y_next, mate):
         pl.semaphore_signal(barrier, inc=1, device_id=dev, device_id_type=MESH)
     for k in range(NX, 128 // 8):
@@ -97,13 +93,14 @@
     loads_scores = load(rs_in, scores, small_sem.at[7])
     loads_hg = load(hg_in, hg, small_sem.at[5])
     loads_lam = load(lam_in, lam, small_sem.at[8])
-    load_wg = load(wg_in.at[0], wgu.at[:, pl.ds(0, FFL)], wsem.at[0])
-    load_wu = load(wu_in.at[0], wgu.at[:, pl.ds(FFL, FFL)], wsem.at[1])
+    load(wg_in.at[0], wgu.at[:, pl.ds(0, FFL)], wsem.at[0])
+    load(wu_in.at[0], wgu.at[:, pl.ds(FFL, FFL)], wsem.at[0])
 
     def wd_cols(yd, c):
         return wd_in.at[0, :, pl.ds(pl.multiple_of((yd * 2 + c) * FEAT, FEAT), FEAT)]
 
-    wd_loads = [load(wd_cols(yd, core), wdx.at[core, yd], wsem.at[2 + yd]) for yd in range(RING)]
+    for yd in range(RING):
+        load(wd_cols(yd, core), wdx.at[core, yd], wsem.at[1])
 
     loads_routes.wait()
     r0, r1 = routes[0:1, :], routes[1:2, :]
@@ -250,8 +247,7 @@
         rdma(wd_cols(yd, 1 - core), wdx.at[core, yd], wdx_s, wdx_r, mate).start()
     for off in ORDER:
         ag_step(2, off)
-    load_wg.wait()
-    load_wu.wait()
+    took(gath, wsem.at[0])
 
     def product(rel, rows):
         terms = []
@@ -327,8 +323,7 @@
     expert(ORDER[0])
     ag_step(3, ORDER[2])
     expert(ORDER[1])
-    for copy in wd_loads:
-        copy.wait()
+    took(wdx.at[0], wsem.at[1])
     took(wdx.at[0], wdx_r)
     ag_step(3, ORDER[3])
     launch(ORDER[0])
@@ -492,7 +487,7 @@
         pltpu.VMEM((SLOTS, ROWS_B), BF16),
         pltpu.VMEM((SLOTS, ROWS_B), BF16),
         dma((9,)),
-        dma((2 + RING,)),
+        dma((2,)),
         pltpu.VMEM(boxes, BF16),
         pltpu.VMEM((3, *boxes), BF16),
         pltpu.VMEM(boxes, BF16),

time: 58.3 us -> 57.9 us (level)
  no operation moved by 1% of the time
where the time goes in v4:
time: 57.9 us; the launch traced here: 57.1 us
  Pallas kernels  54.5 us (94%)
  between operations  1.29 us (2%)
  local copies, waits for them, and re-layouts  1.25 us (2%)
    pallas_call x1, Pallas kernels, local(): pl.pallas_call(kernel, out_shape=(pltpu.VMEM((ROWS_A, VD), BF16), pltpu.V...  54.5 us
    unnamed x2, local copies, waits for them, and re-layouts  1.25 us

profile of v4, /device:TPU:1, one launch (start us, length us, event | category | flops | bytes accessed | tf_op | source)
XLA Modules:
  0.0 57.1 jit_solution(17818147509619937319)
XLA Ops:
  1.3 54.5 %shard_map.131 = (bf16[128,256]{1,0:T(8,128)(2,1)S(1)}, bf16[64,256]{1,0:T(8,128)(2,1)S(1)}) custom-call(bf16[128,256]{1,0:T(8,128)(2,1)} %q_in.1, bf16[128,256]{1,0:T(8,128)(2,1)} %k_in.1, bf16[128,256]{1,0:T(8,128)(2,1)} %v_in.1, f32[1]{0:T(128)S(6)} %copy.18.lam_in, f32[1,256]{1,0:T(1,128)} %bitcast.5, bf16[64,4096]{1,0:T(8,128)(2,1)} %tok_in.1, ...), custom_call_target="tpu_custom_call" | custom-call | tf_op jit(solution)/shard_map/pallas_call | solution.py:523
  55.8 0.6 %copy.16 = bf16[128,256]{1,0:T(8,128)(2,1)} copy(bf16[128,256]{1,0:T(8,128)(2,1)S(1)} %get-tuple-element.2) | data formatting | bytes 131072
  56.4 0.6 %copy.17 = bf16[64,256]{1,0:T(8,128)(2,1)} copy(bf16[64,256]{1,0:T(8,128)(2,1)S(1)} %get-tuple-element.3) | data formatting | bytes 65536

commit v5 on v4

--- a/solution.py
+++ b/solution.py
@@ -25,6 +25,7 @@
 SUB = 4
 SROWS = SLOTS // SUB
 GSRC = N_EP // SUB
+HROWS = SLOTS // SUB // 2
 KSUB = 2
 KROWS = ROWS_A // KSUB
 
@@ -288,20 +289,22 @@
     def rel_of(way, r):
         return r % RING if way == 0 else (RING - r) % RING
 
-    def rs_copy(way, r, off):
+    def rs_copy(way, r, p):
+        rows = pl.ds(p * HROWS, HROWS)
         return rdma(
-            sbuf.at[way, r - 1, rows_of(off)], rbuf.at[way, r - 1, rows_of(off)],
-            rsc_s, rsc_r.at[way, r - 1, off], y_next[way],
+            sbuf.at[way, r - 1, rows], rbuf.at[way, r - 1, rows],
+            rsc_s, rsc_r.at[way, r - 1, p], y_next[way],
         )
 
     def rs_send(way, r, off):
-        rows = slice(off * SROWS, (off + 1) * SROWS)
-        term = zown[rel_of(way, r), rows, :]
-        if r < 3 or (r == 3 and travels(way, off)):
-            rs_copy(way, r + 1, off).wait_recv()
-            term = term + rbuf[way, r, rows, :].astype(F32)
-        sbuf[way, r - 1, rows, :] = term.astype(BF16)
-        rs_copy(way, r, off).start()
+        for p in (2 * off, 2 * off + 1):
+            rows = slice(p * HROWS, (p + 1) * HROWS)
+            term = zown[rel_of(way, r), rows, :]
+            if r < 3 or (r == 3 and travels(way, off)):
+                rs_copy(way, r + 1, p).wait_recv()
+                term = term + rbuf[way, r, rows, :].astype(F32)
+            sbuf[way, r - 1, rows, :] = term.astype(BF16)
+            rs_copy(way, r, p).start()
 
     def own_terms(rows, rels):
         hid0, hid1 = hid[0, rows, :], hid[1, rows, :]
@@ -404,8 +407,9 @@
 
     for off in ORDER:
         rows = slice(off * SROWS, (off + 1) * SROWS)
-        rs_copy(0, 1, off).wait_recv()
-        rs_copy(1, 1, off).wait_recv()
+        for p in (2 * off, 2 * off + 1):
+            rs_copy(0, 1, p).wait_recv()
+            rs_copy(1, 1, p).wait_recv()
         result = zown[0, rows, :] + rbuf[0, 0, rows, :].astype(F32) + rbuf[1, 0, rows, :].astype(F32)
         ebox[off * GSRC:(off + 1) * GSRC] = result.reshape(GSRC, CAP, FEAT).astype(BF16)
         first = group(off)
@@ -514,7 +518,7 @@
         dma, dma((2 + SUB,)),
         dma, dma,
         dma, dma((SUB,)),
-        dma, dma((2, 4, SUB)),
+        dma, dma((2, 4, 2 * SUB)),
         dma, dma,
         dma, dma((NX - 1,)),
         dma, dma((2, 4, KSUB)),

time: 57.9 us -> 58.3 us (level)
  the two profiles are of different devices: /device:TPU:1 before, /device:TPU:24 now
where the time goes in v5:
time: 58.3 us; the launch traced here: 58.2 us
  Pallas kernels  55.7 us (96%)
  between operations  1.29 us (2%)
  local copies, waits for them, and re-layouts  1.25 us (2%)
    pallas_call x1, Pallas kernels, local(): pl.pallas_call(kernel, out_shape=(pltpu.VMEM((ROWS_A, VD), BF16), pltpu.V...  55.7 us
    unnamed x2, local copies, waits for them, and re-layouts  1.25 us

profile of v5, /device:TPU:24, one launch (start us, length us, event | category | flops | bytes accessed | tf_op | source)
XLA Modules:
  0.0 58.2 jit_solution(11239899192959689736)
XLA Ops:
  1.3 55.7 %shard_map.131 = (bf16[128,256]{1,0:T(8,128)(2,1)S(1)}, bf16[64,256]{1,0:T(8,128)(2,1)S(1)}) custom-call(bf16[128,256]{1,0:T(8,128)(2,1)} %q_in.1, bf16[128,256]{1,0:T(8,128)(2,1)} %k_in.1, bf16[128,256]{1,0:T(8,128)(2,1)} %v_in.1, f32[1]{0:T(128)S(6)} %copy.18.lam_in, f32[1,256]{1,0:T(1,128)} %bitcast.5, bf16[64,4096]{1,0:T(8,128)(2,1)} %tok_in.1, ...), custom_call_target="tpu_custom_call" | custom-call | tf_op jit(solution)/shard_map/pallas_call | solution.py:527
  57.0 0.6 %copy.16 = bf16[128,256]{1,0:T(8,128)(2,1)} copy(bf16[128,256]{1,0:T(8,128)(2,1)S(1)} %get-tuple-element.2) | data formatting | bytes 131072
  57.6 0.6 %copy.17 = bf16[64,256]{1,0:T(8,128)(2,1)} copy(bf16[64,256]{1,0:T(8,128)(2,1)S(1)} %get-tuple-element.3) | data formatting | bytes 65536
